TPU v7x, 256 devices: a whole 4x4x8 slice. The times are simulated.
256 devices in a mesh: fs: 32 (over z, x), tp: 8 (over y, core).
Axes of the slice: x: 4, y: 4, z: 8, core: 2. Of those that a mesh axis runs over, the one named last changes fastest.
Arguments:
- tokens: bfloat16 [16384, 2048], P('fs', 'tp'), may hold values from -6 to 6
- pre_gain: float32 [2048], replicated, may hold values from 0.1 to 1.9
- pre_gate: float32 [2048, 2816], P('fs', 'tp'), may hold values from -0.125 to 0.125
- pre_up: float32 [2048, 2816], P('fs', 'tp'), may hold values from -0.125 to 0.125
- pre_down: float32 [2816, 2048], P('fs', 'tp'), may hold values from -0.109375 to 0.109375
- mix_gain: float32 [2048], replicated, may hold values from 0.1 to 1.9
- branch_proj: float32 [2048, 1024], P('fs', 'tp'), may hold values from -0.125 to 0.125
- gate_proj: float32 [2048, 1024], P('fs', 'tp'), may hold values from -0.125 to 0.125
- conv_taps: float32 [4, 1024], P(None, 'tp'), may hold values from -3 to 3
- retain_blocks: float32 [16, 64, 64], P('tp'), may hold values from -0.75 to 0.75
- admit_blocks: float32 [16, 64, 64], P('tp'), may hold values from -0.75 to 0.75
- decay_param: float32 [1024], P('tp'), may hold values from 5 to 8.5
- channel_gain: float32 [1024], replicated, may hold values from 0.1 to 1.9
- out_proj: float32 [1024, 2048], P('fs', 'tp'), may hold values from -0.1875 to 0.1875
- post_gain: float32 [2048], replicated, may hold values from 0.1 to 1.9
- post_gate: float32 [2048, 2816], P('fs', 'tp'), may hold values from -0.125 to 0.125
- post_up: float32 [2048, 2816], P('fs', 'tp'), may hold values from -0.125 to 0.125
- post_down: float32 [2816, 2048], P('fs', 'tp'), may hold values from -0.109375 to 0.109375
Outputs:
- layer_out: bfloat16 [16384, 2048], P('fs', 'tp')
All inputs are finite; a program needn't handle non-finite values.
Results may differ from a plain program's by a relative error of at most 0.012.
Values may be sent and summed in bfloat16 or wider, within the bound.
A program may use at most 64 MiB of HBM per device.

v0:
```python
import jax
import jax.numpy as jnp
from jax import lax
from jax.sharding import Mesh
from jax.sharding import PartitionSpec as P

SEQ_LEN = 128
FS = ("fs_0", "fs_1")


EPSILON = 1e-06
DECAY_SCALE = 8.0


def copy_for_each(x, axis):
    copies = jnp.broadcast_to(x, (lax.axis_size(axis), *x.shape))
    return lax.all_to_all(copies, axis, split_axis=0, concat_axis=0, tiled=True)


def laid_out(parts, dim):
    dims = list(parts.shape[1:])
    dims[dim] *= parts.shape[0]
    return jnp.moveaxis(parts, 0, dim).reshape(dims)


def gather_directly(x, axis, dim):
    parts = copy_for_each(x, axis)
    return laid_out(parts, dim)


def gathered_by_axis(x, axes, dim):
    whole = x
    for number in range(len(axes) - 1, -1, -1):
        whole = lax.all_gather(whole, axes[number], axis=dim, tiled=True)
    return whole


def normalize(values, norm_gain):
    floats = values.astype(jnp.float32)
    scaled = floats * lax.rsqrt(jnp.mean(floats * floats, axis=-1, keepdims=True) + EPSILON)
    return (scaled * norm_gain).astype(jnp.bfloat16)


def combine(earlier, latter):
    keep_early, add_early = earlier
    keep_late, add_late = latter
    return (keep_early * keep_late, keep_late * add_early + add_late)


def widen(residual):
    return gather_directly(residual, "tp", 1)


def contract(operand, stacked):
    return jnp.dot(
        operand,
        gathered_by_axis(stacked.astype(jnp.bfloat16), FS, 0),
        preferred_element_type=jnp.float32,
    )


def feed_forward(residual, norm_gain, gate_matrix, up_matrix, down_matrix):
    normed = normalize(widen(residual), norm_gain)
    products = contract(normed, jnp.concatenate((gate_matrix, up_matrix), axis=1))
    split_at = gate_matrix.shape[1]
    hidden = (jax.nn.silu(products[:, :split_at]) * products[:, split_at:]).astype(jnp.bfloat16)
    all_hidden = lax.all_gather(hidden, "tp", axis=1, tiled=True)
    return (residual.astype(jnp.float32) + 0.5 * contract(all_hidden, down_matrix)).astype(
        jnp.bfloat16
    )


def block_gate(convolved, blocks):
    grouped = convolved.reshape(
        convolved.shape[0], convolved.shape[1], blocks.shape[0], blocks.shape[1]
    )
    mixed = jnp.einsum(
        "sthi,hij->sthj", grouped, blocks.astype(jnp.bfloat16), preferred_element_type=jnp.float32
    )
    return jax.nn.sigmoid(mixed).reshape(convolved.shape)


def recurrent_mixer(
    residual,
    norm_gain,
    branch_matrix,
    gate_matrix,
    conv_taps,
    retain_blocks,
    admit_blocks,
    decay_param,
    channel_gain,
    out_matrix,
):
    normed = normalize(widen(residual), norm_gain)
    products = contract(normed, jnp.concatenate((branch_matrix, gate_matrix), axis=1))
    local_width = branch_matrix.shape[1]
    branch = products[:, :local_width]
    gate_act = products[:, local_width:]
    taps_count = conv_taps.shape[0]
    sequences = residual.shape[0] // SEQ_LEN
    framed = branch.reshape(sequences, SEQ_LEN, local_width)
    padded = jnp.pad(framed, ((0, 0), (taps_count - 1, 0), (0, 0)))
    convolved = jnp.zeros_like(framed)
    for tap_index in range(taps_count):
        convolved = convolved + padded[:, tap_index : tap_index + SEQ_LEN] * conv_taps[tap_index]
    convolved = convolved.astype(jnp.bfloat16)
    retained = block_gate(convolved, retain_blocks)
    admitted = block_gate(convolved, admit_blocks)
    log_keep = -DECAY_SCALE * retained * jax.nn.softplus(-decay_param)
    inject = jnp.sqrt(-jnp.expm1(2.0 * log_keep)) * admitted * convolved.astype(jnp.float32)
    _, states = lax.associative_scan(combine, (jnp.exp(log_keep), inject), axis=1)
    mixed_rows = (states.reshape(residual.shape[0], local_width) * jax.nn.gelu(gate_act)).astype(
        jnp.bfloat16
    )
    all_channels = gather_directly(mixed_rows, "tp", 1)
    mixed_normed = normalize(all_channels, channel_gain)
    return (residual.astype(jnp.float32) + contract(mixed_normed, out_matrix)).astype(jnp.bfloat16)


def local(
    tokens,
    pre_gain,
    pre_gate,
    pre_up,
    pre_down,
    mix_gain,
    branch_proj,
    gate_proj,
    conv_taps,
    retain_blocks,
    admit_blocks,
    decay_param,
    channel_gain,
    out_proj,
    post_gain,
    post_gate,
    post_up,
    post_down,
):
    after_pre = feed_forward(tokens, pre_gain, pre_gate, pre_up, pre_down)
    after_mix = recurrent_mixer(
        after_pre,
        mix_gain,
        branch_proj,
        gate_proj,
        conv_taps,
        retain_blocks,
        admit_blocks,
        decay_param,
        channel_gain,
        out_proj,
    )
    return feed_forward(after_mix, post_gain, post_gate, post_up, post_down)


def solution(mesh):
    torus = Mesh(mesh.devices.reshape(8, 4, mesh.shape["tp"]), ("fs_0", "fs_1", "tp"))
    placed = (
        P(FS, "tp"),
        P(),
        P(FS, "tp"),
        P(FS, "tp"),
        P(FS, "tp"),
        P(),
        P(FS, "tp"),
        P(FS, "tp"),
        P(None, "tp"),
        P("tp", None, None),
        P("tp", None, None),
        P("tp"),
        P(),
        P(FS, "tp"),
        P(),
        P(FS, "tp"),
        P(FS, "tp"),
        P(FS, "tp"),
    )
    return jax.shard_map(local, mesh=torus, in_specs=placed, out_specs=P(FS, "tp"), check_vma=False)
```

profile of v0, /device:TPU:1, one launch (start us, length us, event | category | flops | bytes accessed | tf_op | source)
XLA Modules:
  0.0 431.4 jit_solution(11646481140543656673)
XLA Ops:
  8.4 12.3 %all_gather.42 = bf16[256,704]{1,0:T(8,128)(2,1)} all-gather(bf16[64,704]{1,0:T(8,128)(2,1)S(1)} %pad_maximum_fusion.3), channel_id=1, replica_groups=mesh['fs_0'=8,'fs_1'=4,'tp'=8] {'fs_1'}, dimensions={0}, use_global_device_ids=true | all-gather | bytes 450560 | tf_op jit(solution)/shard_map/all_gather | solution.py:34
  23.4 8.2 %all-to-all-start = ((bf16[8,512,256]{1,2,0:T(8,128)(2,1)}), bf16[8,512,256]{1,2,0:T(8,128)(2,1)S(1)}, u32[]{:S(2)}, u32[]{:S(2)}) async-start(bf16[8,512,256]{1,2,0:T(8,128)(2,1)} %broadcast_in_dim.8), calls=%async_computation | async-start | bytes 4194304 | tf_op jit(solution)/shard_map/all_to_all | solution.py:17
  31.6 10.6 %all_gather.45 = bf16[352,256]{1,0:T(8,128)(2,1)} all-gather(bf16[88,256]{1,0:T(8,128)(2,1)S(1)} %convert_element_type.124), channel_id=1, replica_groups=mesh['fs_0'=8,'fs_1'=4,'tp'=8] {'fs_1'}, dimensions={0}, use_global_device_ids=true | all-gather | bytes 225280 | tf_op jit(solution)/shard_map/all_gather | solution.py:34
  42.2 15.5 %all-to-all-done = bf16[8,512,256]{1,2,0:T(8,128)(2,1)S(1)} async-done(((bf16[8,512,256]{1,2,0:T(8,128)(2,1)}), bf16[8,512,256]{1,2,0:T(8,128)(2,1)S(1)}, u32[]{:S(2)}, u32[]{:S(2)}) %all-to-all-start) | async-done | bytes 2097184 | tf_op jit(solution)/shard_map/all_to_all | solution.py:17
  60.2 10.1 %all-gather.8.cloned.1.call-done = bf16[2048,704]{1,0:T(8,128)(2,1)} async-done(((bf16[256,704]{1,0:T(8,128)(2,1)}), bf16[2048,704]{1,0:T(8,128)(2,1)}) %all-gather.8.cloned.1.call-update) | async-done | bytes 2883600 | tf_op jit(solution)/shard_map/all_gather | solution.py:34
  70.3 4.2 fusion.56
  75.6 10.4 %all_gather.47 = bf16[256,256]{1,0:T(8,128)(2,1)} all-gather(bf16[64,256]{1,0:T(8,128)(2,1)S(1)} %pad_maximum_fusion.5), channel_id=1, replica_groups=mesh['fs_0'=8,'fs_1'=4,'tp'=8] {'fs_1'}, dimensions={0}, use_global_device_ids=true | all-gather | bytes 163840 | tf_op jit(solution)/shard_map/all_gather | solution.py:34
  86.1 20.4 %all-gather.12.cloned.1.call-done = bf16[2816,256]{1,0:T(8,128)(2,1)} async-done(((bf16[352,256]{1,0:T(8,128)(2,1)}), bf16[2816,256]{1,0:T(8,128)(2,1)}) %all-gather.12.cloned.1.call-update) | async-done | bytes 1441808 | tf_op jit(solution)/shard_map/all_gather | solution.py:34
  106.5 34.1 %all-gather.10.cloned.1.call-done = bf16[512,2816]{0,1:T(8,128)(2,1)} async-done(((bf16[512,352]{0,1:T(8,128)(2,1)}), bf16[512,2816]{0,1:T(8,128)(2,1)}) %all-gather.10.cloned.1.call-update) | async-done | bytes 2883600 | tf_op jit(solution)/shard_map/all_gather | solution.py:67
  140.6 3.2 fusion.12
  145.5 3.9 all-to-all-start.1
  149.5 11.1 %all_gather.51 = bf16[256,704]{1,0:T(8,128)(2,1)} all-gather(bf16[64,704]{1,0:T(8,128)(2,1)S(1)} %pad_maximum_fusion.4), channel_id=1, replica_groups=mesh['fs_0'=8,'fs_1'=4,'tp'=8] {'fs_1'}, dimensions={0}, use_global_device_ids=true | all-gather | bytes 450560 | tf_op jit(solution)/shard_map/all_gather | solution.py:34
  160.7 15.0 %all-to-all-done.1 = bf16[8,512,256]{1,2,0:T(8,128)(2,1)S(1)} async-done(((bf16[8,512,256]{1,2,0:T(8,128)(2,1)}), bf16[8,512,256]{1,2,0:T(8,128)(2,1)S(1)}, u32[]{:S(2)}, u32[]{:S(2)}) %all-to-all-start.1) | async-done | bytes 2097184 | tf_op jit(solution)/shard_map/all_to_all | solution.py:17
  178.0 2.6 fusion.57
  182.9 4.6 %slice.212 = f32[4,64,128]{1,2,0:T(8,128)S(1)} slice(f32[4,128,128]{1,2,0:T(8,128)S(1)} %get-tuple-element.6), slice={[0:4:1], [0:127:2], [0:128:1]} | slice | bytes 262144 | tf_op jit(solution)/shard_map/slice | solution.py:112
  187.6 4.5 %slice.213 = f32[4,64,128]{1,2,0:T(8,128)S(1)} slice(f32[4,128,128]{1,2,0:T(8,128)S(1)} %get-tuple-element.6), slice={[0:4:1], [1:128:2], [0:128:1]} | slice | bytes 262144 | tf_op jit(solution)/shard_map/slice | solution.py:112
  192.1 4.5 %slice.211 = f32[4,64,128]{1,2,0:T(8,128)S(1)} slice(f32[4,128,128]{1,2,0:T(8,128)S(1)} %get-tuple-element.5), slice={[0:4:1], [1:128:2], [0:128:1]} | slice | bytes 262144 | tf_op jit(solution)/shard_map/slice | solution.py:112
  196.7 4.5 %slice.215 = f32[4,64,128]{1,2,0:T(8,128)S(1)} slice(f32[4,128,128]{1,2,0:T(8,128)S(1)} %get-tuple-element.5), slice={[0:4:1], [0:127:2], [0:128:1]} | slice | bytes 262144 | tf_op jit(solution)/shard_map/slice | solution.py:112
  245.3 4.5 %slice.259 = f32[4,63,128]{1,2,0:T(8,128)S(1)} slice(f32[4,128,128]{1,2,0:T(8,128)S(1)} %get-tuple-element.6), slice={[0:4:1], [2:128:2], [0:128:1]} | slice | bytes 258048 | tf_op jit(solution)/shard_map/slice | solution.py:112
  249.8 4.5 %slice.210 = f32[4,63,128]{1,2,0:T(8,128)S(1)} slice(f32[4,128,128]{1,2,0:T(8,128)S(1)} %get-tuple-element.5), slice={[0:4:1], [2:128:2], [0:128:1]} | slice | bytes 258048 | tf_op jit(solution)/shard_map/slice | solution.py:112
  276.2 4.6 %pad.61 = f32[4,128,128]{1,2,0:T(8,128)S(1)} pad(f32[4,64,128]{1,2,0:T(8,128)S(1)} %add.195, f32[]{:T(128)} %constant.10.clone.1), padding=0_0_0x1_0_1x0_0_0 | pad | bytes 393220 | tf_op jit(solution)/shard_map/pad | solution.py:112
  281.0 4.5 %pad.60 = f32[4,128,128]{1,2,0:T(8,128)S(1)} pad(f32[4,64,128]{1,2,0:T(8,128)S(1)} %pad_maximum_fusion.2, f32[]{:T(128)} %constant.10.clone.1), padding=0_0_0x0_1_1x0_0_0 | pad | bytes 393220 | tf_op jit(solution)/shard_map/pad | solution.py:112
  287.1 7.7 %all-to-all-start.2 = ((bf16[8,512,128]{1,2,0:T(8,128)(2,1)}), bf16[8,512,128]{1,2,0:T(8,128)(2,1)S(1)}, u32[]{:S(2)}, u32[]{:S(2)}) async-start(bf16[8,512,128]{1,2,0:T(8,128)(2,1)} %broadcast_in_dim.10), calls=%async_computation.2 | async-start | bytes 2097152 | tf_op jit(solution)/shard_map/all_to_all | solution.py:17
  294.8 10.3 %all_gather.49 = bf16[128,256]{1,0:T(8,128)(2,1)S(1)} all-gather(bf16[32,256]{1,0:T(8,128)(2,1)S(1)} %convert_element_type.142), channel_id=1, replica_groups=mesh['fs_0'=8,'fs_1'=4,'tp'=8] {'fs_1'}, dimensions={0}, use_global_device_ids=true | all-gather | bytes 81920 | tf_op jit(solution)/shard_map/all_gather | solution.py:34
  305.0 20.3 %all_gather.50 = bf16[1024,256]{1,0:T(8,128)(2,1)S(1)} all-gather(bf16[128,256]{1,0:T(8,128)(2,1)S(1)} %all_gather.49), channel_id=1, replica_groups=mesh['fs_0'=8,'fs_1'=4,'tp'=8] {'fs_0'}, dimensions={0}, use_global_device_ids=true | all-gather | bytes 589824 | tf_op jit(solution)/shard_map/all_gather | solution.py:34
  328.1 12.1 %all-to-all-start.3 = ((bf16[8,512,256]{1,2,0:T(8,128)(2,1)}), bf16[8,512,256]{1,2,0:T(8,128)(2,1)S(1)}, u32[]{:S(2)}, u32[]{:S(2)}) async-start(bf16[8,512,256]{1,2,0:T(8,128)(2,1)} %broadcast_in_dim.11), calls=%async_computation.3 | async-start | bytes 4194304 | tf_op jit(solution)/shard_map/all_to_all | solution.py:17
  340.2 10.3 %all_gather.54 = bf16[352,256]{1,0:T(8,128)(2,1)} all-gather(bf16[88,256]{1,0:T(8,128)(2,1)S(1)} %convert_element_type.151), channel_id=1, replica_groups=mesh['fs_0'=8,'fs_1'=4,'tp'=8] {'fs_1'}, dimensions={0}, use_global_device_ids=true | all-gather | bytes 225280 | tf_op jit(solution)/shard_map/all_gather | solution.py:34
  350.6 15.8 %all-to-all-done.3 = bf16[8,512,256]{1,2,0:T(8,128)(2,1)S(1)} async-done(((bf16[8,512,256]{1,2,0:T(8,128)(2,1)}), bf16[8,512,256]{1,2,0:T(8,128)(2,1)S(1)}, u32[]{:S(2)}, u32[]{:S(2)}) %all-to-all-start.3) | async-done | bytes 2097184 | tf_op jit(solution)/shard_map/all_to_all | solution.py:17
  368.8 4.3 fusion.58
  374.1 11.7 %all-gather.20.cloned.1.call-done = bf16[2816,256]{1,0:T(8,128)(2,1)} async-done(((bf16[352,256]{1,0:T(8,128)(2,1)}), bf16[2816,256]{1,0:T(8,128)(2,1)}) %all-gather.20.cloned.1.call-update) | async-done | bytes 1441808 | tf_op jit(solution)/shard_map/all_gather | solution.py:34
  385.8 34.4 %all-gather.18.cloned.1.call-done = bf16[512,2816]{0,1:T(8,128)(2,1)} async-done(((bf16[512,352]{0,1:T(8,128)(2,1)}), bf16[512,2816]{0,1:T(8,128)(2,1)}) %all-gather.18.cloned.1.call-update) | async-done | bytes 2883600 | tf_op jit(solution)/shard_map/all_gather | solution.py:67
  420.2 3.9 fusion.11
  (187 shorter events, 88.0 us)
Async XLA Ops:
  6.5 63.8 %all-gather.8.cloned.1.call-start = ((), (), s32[]{:S(2)}) async-start(), calls=%async_computation.4 | async-start | bytes 3538944 | tf_op jit(solution)/shard_map/all_gather | solution.py:34
  23.4 8.2 %copy-start.9 = (f32[88,256]{1,0:T(8,128)S(1)}, f32[88,256]{1,0:T(8,128)}, u32[]{:S(2)}) copy-start(f32[88,256]{1,0:T(8,128)} %param.22) | copy-start | bytes 270340
  23.4 34.4 %all-to-all-start = ((bf16[8,512,256]{1,2,0:T(8,128)(2,1)}), bf16[8,512,256]{1,2,0:T(8,128)(2,1)S(1)}, u32[]{:S(2)}, u32[]{:S(2)}) async-start(bf16[8,512,256]{1,2,0:T(8,128)(2,1)} %broadcast_in_dim.8), calls=%async_computation | async-start | bytes 4194304 | tf_op jit(solution)/shard_map/all_to_all | solution.py:17
  31.5 26.8 %copy-start.14 = (f32[2048]{0:T(1024)S(1)}, f32[2048]{0:T(1024)}, u32[]{:S(2)}) copy-start(f32[2048]{0:T(1024)} %param.19) | copy-start | bytes 24580
  31.5 75.0 %all-gather.12.cloned.1.call-start = ((), (), s32[]{:S(2)}) async-start(), calls=%async_computation.6 | async-start | bytes 1622016 | tf_op jit(solution)/shard_map/all_gather | solution.py:34
  42.2 98.4 %all-gather.10.cloned.1.call-start = ((), (), s32[]{:S(2)}) async-start(), calls=%async_computation.5 | async-start | bytes 3244032 | tf_op jit(solution)/shard_map/all_gather | solution.py:67
  74.5 1.1 copy-start.11
  74.5 1.1 copy-start.12
  74.5 66.1 %copy-start.2 = (bf16[512,256]{1,0:T(8,128)(2,1)S(1)}, bf16[512,256]{1,0:T(8,128)(2,1)}, u32[]{:S(2)}) copy-start(bf16[512,256]{1,0:T(8,128)(2,1)} %param.18) | copy-start | bytes 786436
  75.5 102.5 %all-gather.14.cloned.1.call-start = ((), (), s32[]{:S(2)}) async-start(), calls=%async_computation.7 | async-start | bytes 1179648 | tf_op jit(solution)/shard_map/all_gather | solution.py:34
  143.8 1.7 copy-start.3
  145.4 4.0 copy-start.7
  145.4 4.0 copy-start.8
  145.4 15.2 %copy-start.21 = (f32[128]{0:T(128)S(1)}, f32[128]{0:T(128)}, u32[]{:S(2)}) copy-start(f32[128]{0:T(128)} %param.29) | copy-start | bytes 1540
  145.4 15.2 %copy-start.18 = (f32[4,128]{1,0:T(4,128)S(1)}, f32[4,128]{1,0:T(4,128)}, u32[]{:S(2)}) copy-start(f32[4,128]{1,0:T(4,128)} %param.26) | copy-start | bytes 6148
  145.5 30.2 %all-to-all-start.1 = ((bf16[8,512,256]{1,2,0:T(8,128)(2,1)}), bf16[8,512,256]{1,2,0:T(8,128)(2,1)S(1)}, u32[]{:S(2)}, u32[]{:S(2)}) async-start(bf16[8,512,256]{1,2,0:T(8,128)(2,1)} %broadcast_in_dim.9), calls=%async_computation.1 | async-start | bytes 4194304 | tf_op jit(solution)/shard_map/all_to_all | solution.py:17
  149.4 26.8 %copy-start.15 = (f32[2048]{0:T(1024)S(1)}, f32[2048]{0:T(1024)}, u32[]{:S(2)}) copy-start(f32[2048]{0:T(1024)} %param.23) | copy-start | bytes 24580
  149.4 219.4 %all-gather.16.cloned.1.call-start = ((), (), s32[]{:S(2)}) async-start(), calls=%async_computation.8 | async-start | bytes 3538944 | tf_op jit(solution)/shard_map/all_gather | solution.py:34
  178.0 3.9 copy-start.19
  180.6 1.6 copy-start.20
  262.3 7.2 %copy-start.5 = (f32[4,15,128]{1,2,0:T(8,128)S(1)}, f32[4,15,128]{1,2,0:T(8,128)}, u32[]{:S(2)}) copy-start(f32[4,15,128]{1,2,0:T(8,128)} %slice.222) | copy-start | bytes 92164
  262.3 7.2 %copy-start.6 = (f32[4,15,128]{1,2,0:T(8,128)S(1)}, f32[4,15,128]{1,2,0:T(8,128)}, u32[]{:S(2)}) copy-start(f32[4,15,128]{1,2,0:T(8,128)} %slice.255) | copy-start | bytes 92164
  280.8 4.9 %copy-start.1 = (f32[512,256]{1,0:T(8,128)S(1)}, f32[512,256]{1,0:T(8,128)}, u32[]{:S(2)}) copy-start(f32[512,256]{1,0:T(8,128)} %copy-done) | copy-start | bytes 1572868
  285.7 9.0 %copy-start.13 = (f32[32,256]{1,0:T(8,128)S(1)}, f32[32,256]{1,0:T(8,128)}, u32[]{:S(2)}) copy-start(f32[32,256]{1,0:T(8,128)} %param.31) | copy-start | bytes 98308
  287.1 38.6 %copy-start.17 = (f32[1024]{0:T(1024)S(1)}, f32[1024]{0:T(1024)}, u32[]{:S(2)}) copy-start(f32[1024]{0:T(1024)} %param.30) | copy-start | bytes 12292
  287.1 38.3 %all-to-all-start.2 = ((bf16[8,512,128]{1,2,0:T(8,128)(2,1)}), bf16[8,512,128]{1,2,0:T(8,128)(2,1)S(1)}, u32[]{:S(2)}, u32[]{:S(2)}) async-start(bf16[8,512,128]{1,2,0:T(8,128)(2,1)} %broadcast_in_dim.10), calls=%async_computation.2 | async-start | bytes 2097152 | tf_op jit(solution)/shard_map/all_to_all | solution.py:17
  294.8 31.2 %copy-start.4 = (bf16[512,256]{1,0:T(8,128)(2,1)S(1)}, bf16[512,256]{1,0:T(8,128)(2,1)}, u32[]{:S(2)}) copy-start(bf16[512,256]{1,0:T(8,128)(2,1)} %copy-done.3) | copy-start | bytes 786436
  328.1 12.1 %copy-start.10 = (f32[88,256]{1,0:T(8,128)S(1)}, f32[88,256]{1,0:T(8,128)}, u32[]{:S(2)}) copy-start(f32[88,256]{1,0:T(8,128)} %param.35) | copy-start | bytes 270340
  328.1 38.3 %all-to-all-start.3 = ((bf16[8,512,256]{1,2,0:T(8,128)(2,1)}), bf16[8,512,256]{1,2,0:T(8,128)(2,1)S(1)}, u32[]{:S(2)}, u32[]{:S(2)}) async-start(bf16[8,512,256]{1,2,0:T(8,128)(2,1)} %broadcast_in_dim.11), calls=%async_computation.3 | async-start | bytes 4194304 | tf_op jit(solution)/shard_map/all_to_all | solution.py:17
  340.2 26.7 %copy-start.16 = (f32[2048]{0:T(1024)S(1)}, f32[2048]{0:T(1024)}, u32[]{:S(2)}) copy-start(f32[2048]{0:T(1024)} %param.32) | copy-start | bytes 24580
  340.2 45.6 %all-gather.20.cloned.1.call-start = ((), (), s32[]{:S(2)}) async-start(), calls=%async_computation.10 | async-start | bytes 1622016 | tf_op jit(solution)/shard_map/all_gather | solution.py:34
  350.6 69.6 %all-gather.18.cloned.1.call-start = ((), (), s32[]{:S(2)}) async-start(), calls=%async_computation.9 | async-start | bytes 3244032 | tf_op jit(solution)/shard_map/all_gather | solution.py:67
  (1 other events, 0.8 us)
Sparse Core Ops, SparseCore 0:
  20.9 49.3 all-gather.7
  72.1 34.3 all-gather.11
  108.3 32.2 all-gather.9
  142.2 34.1 all-gather.13
  178.0 47.0 all-gather.15
  350.7 35.0 all-gather.19
  387.6 32.5 all-gather.17
where the time goes:
time: 439 us; the launch traced here: 431 us
  waiting for transfers between devices  157 us (36%)
  local copies, waits for them, and re-layouts  101 us (23%)
  blocking collectives  85.3 us (19%)
  starting transfers between devices  32 us (7%)
  other arithmetic  22 us (5%)
  matrix products  19.2 us (4%)
  between operations  14.8 us (3%)
    all_gather x7, blocking collectives, gathered_by_axis(): whole = lax.all_gather(whole, axes[number], axis=dim, tiled=True)  85.3 us
    all_gather x2, waiting for transfers between devices, feed_forward(): all_hidden = lax.all_gather(hidden, 'tp', axis=1, tiled=True)  68.5 us
    slice x34, local copies, waits for them, and re-layouts, recurrent_mixer(): lax.associative_scan(combine, (jnp.exp(log_keep), inject), axis=1)  65.3 us
    all_to_all x4, waiting for transfers between devices, copy_for_each(): return lax.all_to_all(copies, axis, split_axis=0, concat_axis=0, tiled=True)  46.3 us
    all_gather x5, waiting for transfers between devices, gathered_by_axis(): whole = lax.all_gather(whole, axes[number], axis=dim, tiled=True)  42.3 us
    all_to_all x4, starting transfers between devices, copy_for_each(): return lax.all_to_all(copies, axis, split_axis=0, concat_axis=0, tiled=True)  31.9 us
    pad x12, local copies, waits for them, and re-layouts, recurrent_mixer(): lax.associative_scan(combine, (jnp.exp(log_keep), inject), axis=1)  20.3 us
    dot_general x6, matrix products, contract(): jnp.dot(operand, gathered_by_axis(stacked.astype(jnp.bfloat16), FS, 0), p...  18.7 us
  transfers between devices with their start and end apart: 11, of which 8 were waited for; matrix products, arithmetic and copies ran while one was open for 31% of the time, Pallas kernels for 0%

commit v1 on v0

v1 whole, which is shorter than its diff:
```python
import functools

import jax
import jax.numpy as jnp
from jax import lax
from jax.experimental import pallas as pl
from jax.experimental.pallas import tpu as pltpu
from jax.sharding import Mesh
from jax.sharding import PartitionSpec as P


EPSILON = 1e-06
DECAY_SCALE = 8.0
NZ, NX, NY = 8, 4, 4
TP = 8
SEQ_LEN = 128
ROWS = 512
CHUNKS = ROWS // SEQ_LEN
LANES = 128
BF16, F32 = jnp.bfloat16, jnp.float32
MESH = pl.DeviceIdType.MESH

W1, W2, W3, W4, W5, W6 = "W1", "W2", "W3", "W4", "W5", "W6"
UNIT = {W1: 64, W2: 96, W3: 64, W4: 32, W5: 64, W6: 96}
TILES = {W1: 6, W2: 2, W3: 2, W4: 2, W5: 6, W6: 2}
OFFSET = {}
SLAB = 0
for _name in (W1, W2, W3, W4, W5, W6):
    OFFSET[_name] = SLAB
    SLAB += UNIT[_name] * TILES[_name]

PIECES = (
    (OFFSET[W1], 160, 224, (W1,)),
    (OFFSET[W2], 80, 112, (W2,)),
    (OFFSET[W3], 80, 112, (W3, W4)),
    (OFFSET[W5], 160, 224, (W5,)),
    (OFFSET[W6], 80, 112, (W6,)),
)
PIECE_OF = {W1: 0, W2: 1, W3: 2, W4: 2, W5: 3, W6: 4}
MAX_COPIES = 448

RATE = {"f": 60e3, "b": 33e3, "zf": 50e3, "zb": 40e3, "d": 500e3}
LATENCY = {"link": 2.2, "d": 1.1}
COST = {1: 1.7, 2: 1.0, 3: 1.6, 4: 0.6, 5: 1.7, 6: 1.0}


class Task:
    def __init__(self, name, fn, after=(), needs=(), sends=(), cost=0.05, rank=0):
        self.name, self.fn, self.after, self.needs = name, fn, after, needs
        self.sends, self.cost, self.rank = sends, cost, rank


def ordered(tasks):
    done, arrival, free, now, order = set(), {}, {}, 0.0, []
    left = list(tasks)
    while left:
        best = None
        for task in left:
            if any(a not in done for a in task.after) or any(m not in arrival for m in task.needs):
                continue
            ready = max([arrival[m] for m in task.needs], default=0.0)
            key = (max(ready, now), task.rank, ready)
            if best is None or key < best[0]:
                best = (key, task)
        key, task = best
        now = key[0] + task.cost
        for message, queue, size in task.sends:
            begin = max(free.get(queue, 0.0), now)
            kind = queue if queue in RATE else queue[1]
            end = begin + size / RATE[kind]
            free[queue] = end
            arrival[message] = end + LATENCY["d" if queue == "d" else "link"]
        done.add(task.name)
        left.remove(task)
        order.append(task)
    ordered.estimate = now
    return order


def stable_one_minus_exp(t):
    series = 1.0 - t * (1.0 / 8.0)
    for n in (7.0, 6.0, 5.0, 4.0, 3.0, 2.0):
        series = 1.0 - t * (1.0 / n) * series
    return jnp.where(t < 0.5, t * series, 1.0 - jnp.exp(-t))


def softplus(v):
    e = jnp.exp(-jnp.abs(v))
    u = e / (2.0 + e)
    s = u * u
    total = jnp.zeros_like(s)
    for n in (19, 17, 15, 13, 11, 9, 7, 5, 3, 1):
        total = total * s + 1.0 / n
    return jnp.maximum(v, 0.0) + 2.0 * u * total


def silu(v):
    return v / (1.0 + jnp.exp(-v))


def sigmoid(v):
    return 1.0 / (1.0 + jnp.exp(-v))


def gelu(v):
    return 0.5 * v * (1.0 + jnp.tanh(0.7978845608028654 * (v + 0.044715 * (v * v * v))))


def kernel(
    tokens, pre_gate, pre_up, pre_down, branch_proj, gate_proj, out_proj, post_gate, post_up,
    post_down, pre_gain, mix_gain, channel_gain, post_gain, taps, retain, admit, decay,
    out,
    s_pre_gate, s_pre_up, s_pre_down, s_branch, s_gate, s_out, s_post_gate, s_post_up, s_post_down,
    slab, x1, x2, x3, h1, h2, mixed, wide, spread, blocks, local_sem, send_sem, recv_sem,
):
    z, x, y, c = (lax.axis_index(a) for a in ("z", "x", "y", "c"))
    step = 1 - 2 * c
    me = y * 2 + c

    shards = {
        "pre_gate": (pre_gate, s_pre_gate), "pre_up": (pre_up, s_pre_up),
        "pre_down": (pre_down, s_pre_down), "branch": (branch_proj, s_branch),
        "gate": (gate_proj, s_gate), "out": (out_proj, s_out),
        "post_gate": (post_gate, s_post_gate), "post_up": (post_up, s_post_up),
        "post_down": (post_down, s_post_down),
    }
    loads = {}
    for n, (key, (src, dst)) in enumerate(shards.items()):
        loads[key] = pltpu.make_async_copy(src, dst, local_sem.at[n])
        loads[key].start()
    token_load = pltpu.make_async_copy(tokens, x1.at[me], local_sem.at[len(shards)])
    token_load.start()

    def toward(axis, n, index, distance):
        return {axis: lax.rem(index + distance + n, n)}

    neighbours = [toward(a, n, i, d) for a, n, i in (("z", NZ, z), ("x", NX, x), ("y", NY, y)) for d in (1, -1)]
    neighbours.append({"c": 1 - c})
    barrier = pltpu.get_barrier_semaphore()
    for device in neighbours:
        pl.semaphore_signal(barrier, inc=1, device_id=device, device_id_type=MESH)

    copies = {}

    def send(message, src, dst, device):
        n = len(copies)
        copy = pltpu.make_async_remote_copy(
            src_ref=src, dst_ref=dst, send_sem=send_sem.at[n], recv_sem=recv_sem.at[n],
            device_id=device, device_id_type=MESH,
        )
        copies[message] = copy
        copy.start()

    def arrived(message):
        copies[message].wait_recv()

    lane = lax.broadcasted_iota(jnp.int32, (352, 384), 1)
    row = lax.broadcasted_iota(jnp.int32, (352, 384), 0)
    group = (lane >= 96).astype(jnp.int32) + (lane >= 192).astype(jnp.int32) + (lane >= 288).astype(jnp.int32)
    spread[...] = jnp.where((row == lane - 8 * group) & (lane - 96 * group < 88), 1.0, 0.0).astype(BF16)

    def put(name, tile, value):
        start = OFFSET[name] + UNIT[name] * tile
        slab[z, x, start : start + UNIT[name], :] = value.astype(BF16)

    def build_wide(name, gate_key, up_key):
        for half, key in enumerate((gate_key, up_key)):
            loads[key].wait()
            placed = jnp.dot(shards[key][1][...].astype(BF16), spread[...], preferred_element_type=F32)
            for tile in range(3):
                put(name, half * 3 + tile, placed[:, tile * LANES : (tile + 1) * LANES])

    def build_down(name, key):
        loads[key].wait()
        for tile in range(2):
            value = shards[key][1][:, tile * LANES : (tile + 1) * LANES]
            put(name, tile, jnp.concatenate((value, jnp.zeros((8, LANES), F32)), axis=0))

    def build_mixer():
        loads["branch"].wait()
        put(W3, 0, s_branch[...])
        loads["gate"].wait()
        put(W3, 1, s_gate[...])

    def build_out():
        loads["out"].wait()
        for tile in range(2):
            put(W4, tile, s_out[:, tile * LANES : (tile + 1) * LANES])

    def build_blocks():
        tall = lax.broadcasted_iota(jnp.int32, (LANES, 64), 0)
        flat = lax.broadcasted_iota(jnp.int32, (LANES, 64), 1)
        wide_r = lax.broadcasted_iota(jnp.int32, (64, LANES), 0)
        wide_c = lax.broadcasted_iota(jnp.int32, (64, LANES), 1)
        for n, ref in enumerate((retain, admit)):
            total = jnp.zeros((LANES, LANES), F32)
            for b in range(2):
                left = jnp.where(tall == flat + 64 * b, 1.0, 0.0).astype(BF16)
                right = jnp.where(wide_c == wide_r + 64 * b, 1.0, 0.0).astype(BF16)
                spread_b = jnp.dot(ref[b].astype(BF16), right, preferred_element_type=F32).astype(BF16)
                total = total + jnp.dot(left, spread_b, preferred_element_type=F32)
            blocks[n] = total.astype(BF16)

    builds = {
        W1: lambda: build_wide(W1, "pre_gate", "pre_up"),
        W2: lambda: build_down(W2, "pre_down"),
        W3: build_mixer,
        W4: build_out,
        W5: lambda: build_wide(W5, "post_gate", "post_up"),
        W6: lambda: build_down(W6, "post_down"),
    }

    tasks = []

    def add(*args, **kwargs):
        tasks.append(Task(*args, **kwargs))

    def ring(label, axis, block, size, after, rank):
        n, index = {"x": (NX, x), "z": (NZ, z)}[axis]
        far = n // 2
        near = far - 1
        queue = {"f": axis + "f", "b": axis + "b"}

        def hop(way, k):
            sign = step if way == "f" else -step
            origin = lax.rem(index - sign * (k - 1) + n, n)
            send((label, way, k), block(origin), block(origin), toward(axis, n, index, sign))

        def begin():
            hop("f", 1)
            hop("b", 1)

        add((label, "start"), begin, after=after, rank=rank, cost=0.1,
            sends=[((label, w, 1), queue[w], size) for w in "fb"])
        names = []
        for way, last in (("f", far), ("b", near)):
            previous = (label, "start")
            for k in range(1, last + 1):
                def relay(way=way, k=k, last=last):
                    arrived((label, way, k))
                    if k < last:
                        hop(way, k + 1)
                name = (label, way, k, "relay")
                add(name, relay, after=(previous,), needs=((label, way, k),), rank=rank,
                    sends=[((label, way, k + 1), queue[way], size)] if k < last else [])
                names.append(name)
                previous = name
        return tuple(names)

    piece_done = []
    for p, (first, rows_a, rows_b, needed) in enumerate(PIECES):
        ready = tuple(("build", name) for name in needed)
        for name in needed:
            add(("build", name), builds[name], cost=0.4, rank=p)
        span_a, span_b = slice(first, first + rows_a), slice(first + rows_a, first + rows_a + rows_b)
        size_a, size_b = rows_a * LANES * 2, rows_b * LANES * 2
        a1 = ring((p, "a1"), "x", lambda i, s=span_a: slab.at[z, i, s, :], size_a, ready, p)
        b1 = ring((p, "b1"), "z", lambda i, s=span_b: slab.at[i, x, s, :], size_b, ready, p)
        a2 = ring((p, "a2"), "z", lambda i, s=span_a: slab.at[i, :, s, :], NX * size_a, a1, p)
        b2 = ring((p, "b2"), "x", lambda i, s=span_b: slab.at[:, i, s, :], NZ * size_b, b1, p)
        piece_done.append(a2 + b2)
    for task in tasks:
        if task.name[-1] == "start" and task.name[0][0] > 0 and task.name[0][1] in ("a1", "b1"):
            task.after = task.after + (((task.name[0][0] - 1, task.name[0][1][0] + "2"), "start"),)

    held = {1: (x1, 256), 2: (h1, 384), 3: (x2, 256), 4: (mixed, 128), 5: (x3, 256), 6: (h2, 384)}

    def share(stage, chunk, slot, hops):
        ref = held[stage][0].at[slot, chunk * SEQ_LEN : (chunk + 1) * SEQ_LEN, :]
        for tag, device in hops:
            send((stage, chunk, tag), ref, ref, device)

    up, down, partner = toward("y", NY, y, step), toward("y", NY, y, -step), {"c": 1 - c}

    def slot_at(distance):
        return lax.rem(y + distance + NY, NY) * 2 + c

    def share_own(stage, chunk):
        share(stage, chunk, me, ((("f", 1), up), (("b", 1), down), (("d", 0), partner)))

    def share_tasks(stage, chunk):
        size = SEQ_LEN * held[stage][1] * 2
        rank = -1

        def first():
            arrived((stage, chunk, ("f", 1)))
            share(stage, chunk, slot_at(-step), ((("f", 2), up), (("d", 1), partner)))

        def second():
            arrived((stage, chunk, ("b", 1)))
            share(stage, chunk, slot_at(step), ((("d", 2), partner),))

        def third():
            arrived((stage, chunk, ("f", 2)))
            share(stage, chunk, slot_at(2), ((("d", 3), partner),))

        key = (stage, chunk)
        add((key, "first"), first, needs=((stage, chunk, ("f", 1)),), rank=rank,
            sends=[((stage, chunk, ("f", 2)), "yf", size), ((stage, chunk, ("d", 1)), "d", size)])
        add((key, "second"), second, after=((key, "first"),), needs=((stage, chunk, ("b", 1)),), rank=rank,
            sends=[((stage, chunk, ("d", 2)), "d", size)])
        add((key, "third"), third, after=((key, "second"),), needs=((stage, chunk, ("f", 2)),), rank=rank,
            sends=[((stage, chunk, ("d", 3)), "d", size)])

    def own_sends(stage, chunk):
        size = SEQ_LEN * held[stage][1] * 2
        return [((stage, chunk, ("f", 1)), "yf", size), ((stage, chunk, ("b", 1)), "yb", size),
                ((stage, chunk, ("d", 0)), "d", size)]

    def rows_of(chunk):
        return slice(chunk * SEQ_LEN, (chunk + 1) * SEQ_LEN)

    def weight(name, first, count):
        unit = UNIT[name]
        parts = []
        for tile in range(first, first + count):
            start = OFFSET[name] + unit * tile
            parts.append(slab[:, :, start : start + unit, :].reshape(NZ * NX * unit, LANES))
        return jnp.concatenate(parts, axis=1)

    def scaled(ref, chunk, gain, width):
        squares = jnp.zeros((SEQ_LEN, LANES), F32)
        for slot in range(TP):
            value = ref[slot, rows_of(chunk), :].astype(F32)
            wide[:, slot * width : (slot + 1) * width] = (
                value * gain[:, slot * width : (slot + 1) * width]
            ).astype(BF16)
            square = value * value
            for lane_tile in range(width // LANES):
                squares = squares + square[:, lane_tile * LANES : (lane_tile + 1) * LANES]
        mean = jnp.sum(squares, axis=1, keepdims=True) * (1.0 / (TP * width))
        return lax.rsqrt(mean + EPSILON)

    def product(lhs, name, first, count):
        return jnp.dot(lhs, weight(name, first, count), preferred_element_type=F32)

    def up_stage(source, gain, name, target):
        def run(chunk):
            factor = scaled(source, chunk, gain, 256)
            lhs = wide[...]
            p0 = product(lhs, name, 0, 2) * factor
            p1 = product(lhs, name, 2, 2) * factor
            p2 = product(lhs, name, 4, 2) * factor
            gates = (p0[:, :LANES], p0[:, LANES:], p1[:, :LANES])
            ups = (p1[:, LANES:], p2[:, :LANES], p2[:, LANES:])
            for tile in range(3):
                target[me, rows_of(chunk), tile * LANES : (tile + 1) * LANES] = (
                    silu(gates[tile]) * ups[tile]
                ).astype(BF16)
        return run

    def down_stage(source, name, residual, finish):
        def run(chunk):
            lhs = jnp.concatenate([source[slot, rows_of(chunk), :] for slot in range(TP)], axis=1)
            total = product(lhs, name, 0, 2)
            finish(chunk, (residual[me, rows_of(chunk), :].astype(F32) + 0.5 * total).astype(BF16))
        return run

    def finish_into(target):
        def finish(chunk, value):
            target[me, rows_of(chunk), :] = value
        return finish

    def finish_out(chunk, value):
        out[rows_of(chunk), :] = value

    def mix_stage(chunk):
        factor = scaled(x2, chunk, mix_gain, 256)
        both = product(wide[...], W3, 0, 2) * factor
        branch, gate_act = both[:, :LANES], both[:, LANES:]
        time = lax.broadcasted_iota(jnp.int32, (SEQ_LEN, LANES), 0)

        def earlier(value, k, fill):
            return jnp.where(time >= k, pltpu.roll(value, k, 0), fill)

        convolved = jnp.zeros((SEQ_LEN, LANES), F32)
        for k in range(4):
            lag = 3 - k
            shifted = branch if lag == 0 else earlier(branch, lag, 0.0)
            convolved = convolved + shifted * taps[k : k + 1, :]
        convolved = convolved.astype(BF16)
        retained = sigmoid(jnp.dot(convolved, blocks[0], preferred_element_type=F32))
        admitted = sigmoid(jnp.dot(convolved, blocks[1], preferred_element_type=F32))
        rate = DECAY_SCALE * softplus(-decay[...]) * retained
        add_now = jnp.sqrt(stable_one_minus_exp(2.0 * rate)) * admitted * convolved.astype(F32)
        keep = jnp.exp(-rate)
        k = 1
        while k < SEQ_LEN:
            add_now = keep * earlier(add_now, k, 0.0) + add_now
            if 2 * k < SEQ_LEN:
                keep = keep * earlier(keep, k, 1.0)
            k *= 2
        mixed[me, rows_of(chunk), :] = (add_now * gelu(gate_act)).astype(BF16)

    def out_stage(chunk):
        factor = scaled(mixed, chunk, channel_gain, 128)
        total = product(wide[:, : TP * LANES], W4, 0, 2) * factor
        x3[me, rows_of(chunk), :] = (x2[me, rows_of(chunk), :].astype(F32) + total).astype(BF16)

    stages = {
        1: (W1, up_stage(x1, pre_gain, W1, h1)),
        2: (W2, down_stage(h1, W2, x1, finish_into(x2))),
        3: (W3, mix_stage),
        4: (W4, out_stage),
        5: (W5, up_stage(x3, post_gain, W5, h2)),
        6: (W6, down_stage(h2, W6, x3, finish_out)),
    }

    def enter():
        token_load.wait()
        pl.semaphore_wait(barrier, len(neighbours))

    add(("build", "blocks"), build_blocks, cost=0.3, rank=3, after=(("compute", 1, 0),))
    add(("enter",), enter, after=(("build", W1),), rank=-5)
    for task in tasks:
        if task.name == ((0, "a1"), "start") or task.name == ((0, "b1"), "start"):
            task.after = task.after + (("enter",),)
        if task.name[0] == "build" and task.name[1] in (W2, W3, W4, W5, W6):
            task.after = task.after + (((0, "b1"), "start"), ((0, "a1"), "start"))
    for chunk in range(CHUNKS):
        add(("share", 1, chunk), functools.partial(share_own, 1, chunk),
            after=(("enter",),) if chunk == 0 else (("share", 1, chunk - 1),), sends=own_sends(1, chunk), rank=1)
    for stage in range(1, 7):
        for chunk in range(CHUNKS):
            share_tasks(stage, chunk)
            name, run = stages[stage]

            def compute(stage=stage, chunk=chunk, run=run):
                for n in range(4):
                    arrived((stage, chunk, ("d", n)))
                run(chunk)
                if stage < 6:
                    share_own(stage + 1, chunk)

            after = piece_done[PIECE_OF[name]] + (((stage, chunk), "third"),)
            if chunk:
                after = after + (("compute", stage, chunk - 1),)
            if stage == 3:
                after = after + (("build", "blocks"),)
            add(("compute", stage, chunk), compute, after=after, rank=2, cost=COST[stage],
                needs=tuple((stage, chunk, ("d", n)) for n in range(4)),
                sends=own_sends(stage + 1, chunk) if stage < 6 else [])

    for task in ordered(tasks):
        task.fn()
    for copy in copies.values():
        copy.wait_send()


def layer(
    tokens, pre_gain, pre_gate, pre_up, pre_down, mix_gain, branch_proj, gate_proj, conv_taps,
    retain_blocks, admit_blocks, decay_param, channel_gain, out_proj, post_gain, post_gate,
    post_up, post_down,
):
    large = (tokens, pre_gate, pre_up, pre_down, branch_proj, gate_proj, out_proj, post_gate, post_up, post_down)
    small = (
        pre_gain.reshape(1, -1), mix_gain.reshape(1, -1), channel_gain.reshape(1, -1),
        post_gain.reshape(1, -1), conv_taps, retain_blocks, admit_blocks, decay_param.reshape(1, -1),
    )
    return pl.pallas_call(
        kernel,
        out_shape=jax.ShapeDtypeStruct(tokens.shape, tokens.dtype),
        in_specs=[pl.BlockSpec(memory_space=pl.ANY)] * len(large)
        + [pl.BlockSpec(memory_space=pltpu.VMEM)] * len(small),
        out_specs=pl.BlockSpec(memory_space=pltpu.VMEM),
        scratch_shapes=[pltpu.VMEM(a.shape, F32) for a in large[1:]]
        + [
            pltpu.VMEM((NZ, NX, SLAB, LANES), BF16),
            pltpu.VMEM((TP, ROWS, 256), BF16),
            pltpu.VMEM((TP, ROWS, 256), BF16),
            pltpu.VMEM((TP, ROWS, 256), BF16),
            pltpu.VMEM((TP, ROWS, 384), BF16),
            pltpu.VMEM((TP, ROWS, 384), BF16),
            pltpu.VMEM((TP, ROWS, 128), BF16),
            pltpu.VMEM((SEQ_LEN, 2048), BF16),
            pltpu.VMEM((352, 384), BF16),
            pltpu.VMEM((2, LANES, LANES), BF16),
            pltpu.SemaphoreType.DMA((len(large),)),
            pltpu.SemaphoreType.DMA((MAX_COPIES,)),
            pltpu.SemaphoreType.DMA((MAX_COPIES,)),
        ],
        compiler_params=pltpu.CompilerParams(
            collective_id=0, has_side_effects=True, vmem_limit_bytes=56 * 1024 * 1024
        ),
        name="layer",
    )(*large, *small)


def solution(mesh):
    torus = Mesh(mesh.devices.reshape(NZ, NX, NY, 2), ("z", "x", "y", "c"))
    fs, tp = ("z", "x"), ("y", "c")
    split = P(fs, tp)
    placed = (
        split, P(), split, split, split, P(), split, split, P(None, tp), P(tp, None, None),
        P(tp, None, None), P(tp), P(), split, P(), split, split, split,
    )
    return jax.shard_map(layer, mesh=torus, in_specs=placed, out_specs=split, check_vma=False)
```

time: 439 us -> 138 us (0.31); the launches traced: 431 us -> 138 us
  waiting for transfers between devices: 157 us -> 0 us
  Pallas kernels: 0 us -> 136 us
  local copies, waits for them, and re-layouts: 101 us -> 1.67 us
  blocking collectives: 85.3 us -> 0 us
  starting transfers between devices: 32 us -> 0 us
  other arithmetic: 22 us -> 0 us
  matrix products: 19.2 us -> 0 us
  between operations: 14.8 us -> 0.01 us
    pallas_call x0 -> x1, Pallas kernels: none -> 136 us  [layer(): pl.pallas_call(kernel, out_shape=jax.ShapeDtypeStruct(tokens.shape, token...]
    all_gather x7 -> x0, waiting for transfers between devices: 111 us -> none  [the longest x2 68.5 us: feed_forward(): all_hidden = lax.all_gather(hidden, 'tp', axis=1, tiled=True)]
    all_gather x7 -> x0, blocking collectives: 85.3 us -> none  [gathered_by_axis(): whole = lax.all_gather(whole, axes[number], axis=dim, tiled=True)]
    slice x35 -> x0, local copies, waits for them, and re-layouts: 65.3 us -> none  [the longest x34 65.3 us: recurrent_mixer(): lax.associative_scan(combine, (jnp.exp(log_keep), inject), axis=1)]
    all_to_all x4 -> x0, waiting for transfers between devices: 46.3 us -> none  [copy_for_each(): return lax.all_to_all(copies, axis, split_axis=0, concat_axis=0, tiled=True)]
    all_to_all x4 -> x0, starting transfers between devices: 31.9 us -> none  [copy_for_each(): return lax.all_to_all(copies, axis, split_axis=0, concat_axis=0, tiled=True)]
    pad x12 -> x0, local copies, waits for them, and re-layouts: 20.3 us -> none  [recurrent_mixer(): lax.associative_scan(combine, (jnp.exp(log_keep), inject), axis=1)]
    dot_general x8 -> x0, matrix products: 19.2 us -> none  [the longest x6 18.7 us: contract(): jnp.dot(operand, gathered_by_axis(stacked.astype(jnp.bfloat16), FS, 0), p...]
  transfers between devices with their start and end apart: 11 -> 0, of which waited for: 8 -> 0; matrix products, arithmetic and copies ran while one was open for 31% -> 0% of each run, Pallas kernels for 0% -> 0%
where the time goes in v1:
time: 138 us
  Pallas kernels  136 us (99%)
  local copies, waits for them, and re-layouts  1.67 us (1%)
    pallas_call x1, Pallas kernels, layer(): pl.pallas_call(kernel, out_shape=jax.ShapeDtypeStruct(tokens.shape, token...  136 us

profile of v1, /device:TPU:1, one launch (start us, length us, event | category | flops | bytes accessed | tf_op | source)
XLA Modules:
  0.0 137.6 jit_solution(15665951183822195173)
XLA Ops:
  0.0 136.0 %layer.1 = bf16[512,256]{1,0:T(8,128)(2,1)} custom-call(bf16[512,256]{1,0:T(8,128)(2,1)} %tokens.1, f32[64,352]{1,0:T(8,128)} %pre_gate.1, f32[64,352]{1,0:T(8,128)} %pre_up.1, f32[88,256]{1,0:T(8,128)} %pre_down.1, f32[64,128]{1,0:T(8,128)} %branch_proj.1, f32[64,128]{1,0:T(8,128)} %gate_proj.1, f32[32,256]{1,0:T(8,128)} %out_proj.1, f32[64,352]{1,0:T(8,128)} %post_gate.1, ...), custom_call_target="tpu_custom_call" | custom-call | tf_op jit(solution)/shard_map/layer/pallas_call | solution.py:460
  136.0 1.7 %copy.20 = bf16[512,256]{1,0:T(8,128)(2,1)} copy(bf16[512,256]{1,0:T(8,128)(2,1)} %layer.1) | data formatting | bytes 524288

commit v2 on v1

v2 whole, which is shorter than its diff:
```python
import functools

import jax
import jax.numpy as jnp
from jax import lax
from jax.experimental import pallas as pl
from jax.experimental.pallas import tpu as pltpu
from jax.sharding import Mesh
from jax.sharding import PartitionSpec as P


EPSILON = 1e-06
DECAY_SCALE = 8.0
NZ, NX, NY = 8, 4, 4
TP = 8
SEQ_LEN = 128
ROWS = 512
CHUNKS = ROWS // SEQ_LEN
LANES = 128
BF16, F32 = jnp.bfloat16, jnp.float32
MESH = pl.DeviceIdType.MESH

W1, W2, W3, W4, W5, W6 = "W1", "W2", "W3", "W4", "W5", "W6"
UNIT = {W1: 64, W2: 96, W3: 64, W4: 32, W5: 64, W6: 96}
TILES = {W1: 6, W2: 2, W3: 2, W4: 2, W5: 6, W6: 2}
OFFSET = {}
SLAB = 0
for _name in (W1, W2, W3, W4, W5, W6):
    OFFSET[_name] = SLAB
    SLAB += UNIT[_name] * TILES[_name]

FINE_A, FINE_B = ((0,), (1,), (2,)), ((0,), (1,), (2,), (3,), (4,))
COARSE_A, COARSE_B = ((0, 1, 2),), ((0, 1), (2, 3, 4))
PIECES = (
    ("1a", OFFSET[W1], 48, 80, (W1,), FINE_A, FINE_B),
    ("1b", OFFSET[W1] + 128, 48, 80, (W1,), FINE_A, FINE_B),
    ("1c", OFFSET[W1] + 256, 48, 80, (W1,), FINE_A, FINE_B),
    ("2", OFFSET[W2], 80, 112, (W2,), COARSE_A, COARSE_B),
    ("34", OFFSET[W3], 80, 112, (W3, W4), COARSE_A, COARSE_B),
    ("5", OFFSET[W5], 160, 224, (W5,), COARSE_A, COARSE_B),
    ("6", OFFSET[W6], 80, 112, (W6,), COARSE_A, COARSE_B),
)

HALVES, QUARTERS = ((0, 256), (256, 256)), tuple((n * SEQ_LEN, SEQ_LEN) for n in range(CHUNKS))
UNITS = {
    1: tuple((r, n, 0, 256) for r, n in QUARTERS),
    2: tuple((r, n, t * 128, 128) for t in range(2) for r, n in HALVES) + tuple((r, n, 256, 128) for r, n in QUARTERS),
    3: tuple((r, n, 0, 256) for r, n in QUARTERS),
    4: tuple((r, n, 0, 128) for r, n in QUARTERS),
    5: tuple((r, n, 0, 256) for r, n in QUARTERS),
    6: tuple((r, n, 0, 384) for r, n in QUARTERS),
}

SEMS = 320
LINK_RATE, CHIP_RATE = 91e3, 500e3
LINK_LATENCY, CHIP_LATENCY = 1.8, 1.0
BACKLOG = 60e3
COST = {"norm": 0.25, "tile": 0.2, 2: 0.55, 3: 0.8, 4: 0.3, 6: 0.55}


class Task:
    def __init__(self, name, fn, after=(), needs=(), sends=(), cost=0.05, rank=0, gate=None):
        self.name, self.fn, self.after, self.needs = name, fn, tuple(after), tuple(needs)
        self.sends, self.cost, self.rank, self.gate = tuple(sends), cost, rank, gate


class Links:
    def __init__(self):
        self.now, self.queues, self.arrival = 0.0, {}, {}

    def flows(self):
        found = []
        for axis in "xyz":
            heads = [q for q in (axis + "f", axis + "b") if self.queues.get(q)]
            found += [(q, LINK_RATE / len(heads), LINK_LATENCY) for q in heads]
        if self.queues.get("d"):
            found.append(("d", CHIP_RATE, CHIP_LATENCY))
        return found

    def advance(self, until):
        while True:
            flows = self.flows()
            step = min([self.queues[q][0][1] / rate for q, rate, _ in flows], default=1e9)
            if self.now + step > until:
                for q, rate, _ in flows:
                    self.queues[q][0][1] -= rate * (until - self.now)
                self.now = until
                return
            self.now += step
            for q, rate, latency in flows:
                head = self.queues[q][0]
                head[1] -= rate * step
                if head[1] <= 1e-3:
                    self.queues[q].pop(0)
                    self.arrival[head[0]] = self.now + latency

    def next_event(self):
        times = [t for t in self.arrival.values() if t > self.now + 1e-9]
        times += [self.now + self.queues[q][0][1] / rate + 1e-6 for q, rate, _ in self.flows()]
        return min(times)

    def backlog(self, axis):
        return sum(size for q in (axis + "f", axis + "b") for _, size in self.queues.get(q, ()))


def ordered(tasks):
    links, done, order, left = Links(), set(), [], list(tasks)
    waiting = {}
    trace = []
    while left:
        best = None
        for task in left:
            if not all(a in done for a in task.after):
                continue
            ready = 0.0
            for m in task.needs:
                ready = max(ready, links.arrival.get(m, 1e9))
            if ready > links.now or (task.gate and links.backlog(task.gate) > BACKLOG):
                continue
            if best is None or (task.rank, ready) < best[0]:
                best = ((task.rank, ready), task)
        if best is None:
            links.advance(links.next_event())
            continue
        task = best[1]
        trace.append((links.now, task.name))
        links.advance(links.now + task.cost)
        for message, queue, size in task.sends:
            links.queues.setdefault(queue, []).append([message, size])
        done.add(task.name)
        left.remove(task)
        order.append(task)
    ordered.trace, ordered.end = trace, links.now
    return order


def stable_one_minus_exp(t):
    series = 1.0 - t * (1.0 / 8.0)
    for n in (7.0, 6.0, 5.0, 4.0, 3.0, 2.0):
        series = 1.0 - t * (1.0 / n) * series
    return jnp.where(t < 0.5, t * series, 1.0 - jnp.exp(-t))


def softplus(v):
    e = jnp.exp(-jnp.abs(v))
    u = e / (2.0 + e)
    s = u * u
    total = jnp.zeros_like(s)
    for n in (19, 17, 15, 13, 11, 9, 7, 5, 3, 1):
        total = total * s + 1.0 / n
    return jnp.maximum(v, 0.0) + 2.0 * u * total


def silu(v):
    return v / (1.0 + jnp.exp(-v))


def sigmoid(v):
    return 1.0 / (1.0 + jnp.exp(-v))


def gelu(v):
    return 0.5 * v * (1.0 + jnp.tanh(0.7978845608028654 * (v + 0.044715 * (v * v * v))))


def kernel(
    tokens, pre_gate, pre_up, pre_down, branch_proj, gate_proj, out_proj, post_gate, post_up,
    post_down, pre_gain, mix_gain, channel_gain, post_gain, taps, retain, admit, decay,
    out,
    s_pre_gate, s_pre_up, s_pre_down, s_branch, s_gate, s_out, s_post_gate, s_post_up, s_post_down,
    slab, x1, x2, x3, h1, h2, mixed, wide, factors, spread, blocks, local_sem, sems,
):
    z, x, y, c = (lax.axis_index(a) for a in ("z", "x", "y", "c"))
    step = 1 - 2 * c
    me = y * 2 + c

    shards = {
        "pre_gate": (pre_gate, s_pre_gate), "pre_up": (pre_up, s_pre_up),
        "pre_down": (pre_down, s_pre_down), "branch": (branch_proj, s_branch),
        "gate": (gate_proj, s_gate), "out": (out_proj, s_out),
        "post_gate": (post_gate, s_post_gate), "post_up": (post_up, s_post_up),
        "post_down": (post_down, s_post_down),
    }
    loads = {}
    for n, (key, (src, dst)) in enumerate(shards.items()):
        loads[key] = pltpu.make_async_copy(src, dst, local_sem.at[n])
        loads[key].start()
    token_load = pltpu.make_async_copy(tokens, x1.at[me], local_sem.at[len(shards)])
    token_load.start()

    def toward(axis, n, index, distance):
        return {axis: lax.rem(index + distance + n, n)}

    neighbours = [toward(a, n, i, d) for a, n, i in (("z", NZ, z), ("x", NX, x), ("y", NY, y)) for d in (1, -1)]
    neighbours.append({"c": 1 - c})
    barrier = pltpu.get_barrier_semaphore()
    for device in neighbours:
        pl.semaphore_signal(barrier, inc=1, device_id=device, device_id_type=MESH)

    used = {"recv": 0}
    recv_of, drains = {}, []

    def take():
        used["recv"] += 1
        return sems.at[used["recv"] - 1]

    def receipt(message):
        if message not in recv_of:
            recv_of[message] = take()
        return recv_of[message]

    def send(message, send_sem, ref, device):
        pltpu.make_async_remote_copy(
            src_ref=ref, dst_ref=ref, send_sem=send_sem, recv_sem=receipt(message),
            device_id=device, device_id_type=MESH,
        ).start()

    def await_bytes(ref, sem):
        pltpu.make_async_copy(ref, ref, sem).wait()

    lane = lax.broadcasted_iota(jnp.int32, (352, 384), 1)
    row = lax.broadcasted_iota(jnp.int32, (352, 384), 0)
    group = (lane >= 96).astype(jnp.int32) + (lane >= 192).astype(jnp.int32) + (lane >= 288).astype(jnp.int32)
    spread[...] = jnp.where((row == lane - 8 * group) & (lane - 96 * group < 88), 1.0, 0.0).astype(BF16)

    def put(name, tile, value):
        start = OFFSET[name] + UNIT[name] * tile
        slab[z, x, start : start + UNIT[name], :] = value.astype(BF16)

    def build_wide(name, gate_key, up_key):
        for half, key in enumerate((gate_key, up_key)):
            loads[key].wait()
            placed = jnp.dot(shards[key][1][...].astype(BF16), spread[...], preferred_element_type=F32)
            for tile in range(3):
                put(name, half + 2 * tile, placed[:, tile * LANES : (tile + 1) * LANES])

    def build_down(name, key):
        loads[key].wait()
        for tile in range(2):
            value = shards[key][1][:, tile * LANES : (tile + 1) * LANES]
            put(name, tile, jnp.concatenate((value, jnp.zeros((8, LANES), F32)), axis=0))

    def build_mixer():
        loads["branch"].wait()
        put(W3, 0, s_branch[...])
        loads["gate"].wait()
        put(W3, 1, s_gate[...])

    def build_out():
        loads["out"].wait()
        for tile in range(2):
            put(W4, tile, s_out[:, tile * LANES : (tile + 1) * LANES])

    def build_blocks():
        tall = lax.broadcasted_iota(jnp.int32, (LANES, 64), 0)
        flat = lax.broadcasted_iota(jnp.int32, (LANES, 64), 1)
        wide_r = lax.broadcasted_iota(jnp.int32, (64, LANES), 0)
        wide_c = lax.broadcasted_iota(jnp.int32, (64, LANES), 1)
        for n, ref in enumerate((retain, admit)):
            total = jnp.zeros((LANES, LANES), F32)
            for b in range(2):
                left = jnp.where(tall == flat + 64 * b, 1.0, 0.0).astype(BF16)
                right = jnp.where(wide_c == wide_r + 64 * b, 1.0, 0.0).astype(BF16)
                spread_b = jnp.dot(ref[b].astype(BF16), right, preferred_element_type=F32).astype(BF16)
                total = total + jnp.dot(left, spread_b, preferred_element_type=F32)
            blocks[n] = total.astype(BF16)

    builds = {
        W1: lambda: build_wide(W1, "pre_gate", "pre_up"),
        W2: lambda: build_down(W2, "pre_down"),
        W3: build_mixer,
        W4: build_out,
        W5: lambda: build_wide(W5, "post_gate", "post_up"),
        W6: lambda: build_down(W6, "post_down"),
    }

    tasks = []

    def add(*args, **kwargs):
        tasks.append(Task(*args, **kwargs))

    def ring(label, axis, groups, block, blocks_of, rank, size):
        n, index = {"x": (NX, x), "z": (NZ, z)}[axis]
        far = n // 2
        send_sem = take()
        total = n - 1
        count = sum(len(group) for group in groups)
        drains.append((blocks_of(total, count), send_sem))
        starts = []
        for g, group in enumerate(groups):
            width = len(group)

            def hop(way, k, group=group, g=g):
                sign = step if way == "f" else -step
                origin = lax.rem(index - sign * (k - 1) + n, n)
                for member in group:
                    ref = block(origin, member)
                    send((label, g, k), send_sem, ref, toward(axis, n, index, sign))

            def queued(k, g=g, width=width):
                ways = "fb" if k < far else "f"
                return [((label, g, k, way), axis + way, size * width) for way in ways]

            names = []
            for k in range(1, far + 1):
                def relay(k=k, hop=hop, g=g, width=width):
                    await_bytes(blocks_of(2 if k < far else 1, width), recv_of[(label, g, k)])
                    if k < far:
                        hop("f", k + 1)
                    if k < far - 1:
                        hop("b", k + 1)
                names.append((label, g, k))
                needs = [m for m, _, _ in queued(k)]
                starts_k = relay
                ring_tasks[(label, g, k)] = Task(
                    (label, g, k), relay, after=((label, g, k - 1),), needs=needs, rank=rank,
                    sends=queued(k + 1) if k < far else (), cost=0.07)

            def begin(hop=hop):
                hop("f", 1)
                hop("b", 1)

            starts.append((begin, queued(1), names))
        return starts

    ring_tasks = {}
    piece_done = {}
    for p, (label, first, rows_a, rows_b, needed, groups_a, groups_b) in enumerate(PIECES):
        for name in needed:
            if not any(task.name == ("build", name) for task in tasks):
                add(("build", name), builds[name], cost=0.4 if name == W5 else 0.1, rank=p)
        span_a, span_b = slice(first, first + rows_a), slice(first + rows_a, first + rows_a + rows_b)
        size_a, size_b = rows_a * LANES * 2, rows_b * LANES * 2

        def bytes_a(ways, width, s=span_a):
            return slab.at[pl.ds(0, ways), pl.ds(0, width), s, :]

        def bytes_b(ways, width, s=span_b):
            return slab.at[pl.ds(0, width), pl.ds(0, ways), s, :]

        def first_ring(part, axis, block, size, blocks_of, second, groups):
            n = {"x": NX, "z": NZ}[axis]
            far = n // 2
            [(begin, queued, names)] = ring((label, part, axis), axis, ((None,),), block, blocks_of, p, size)
            key = (label, part, axis, "start")
            ready = tuple(("build", name) for name in needed) + (("enter",),)
            starters = {}
            for g, group in enumerate(groups):
                starters.setdefault(group[-1], []).append(g)

            def launch(k):
                for g in starters.get(k, ()):
                    second[g][0]()

            def launch_sends(k):
                return [m for g in starters.get(k, ()) for m in second[g][1]]

            def starting():
                begin()
                launch(0)

            add(key, starting, after=ready, rank=p, sends=list(queued) + launch_sends(0), cost=0.1, gate=axis)
            previous, last = key, None
            for k, name in enumerate(names, 1):
                task = ring_tasks[name]

                def run(inner=task.fn, k=k):
                    inner()
                    launch(k)

                add(name, run, after=(previous,), needs=task.needs, rank=p, cost=0.1,
                    sends=task.sends + tuple(launch_sends(k)))
                previous = name
            ends = []
            for g, group in enumerate(groups):
                begun = key if group[-1] == 0 else names[group[-1] - 1]
                for k, name in enumerate(second[g][2], 1):
                    task = ring_tasks[name]
                    add(name, task.fn, after=(begun if k == 1 else second[g][2][k - 2],), needs=task.needs,
                        rank=p, sends=task.sends, cost=0.07)
                ends.append(second[g][2][-1])
            return (previous,) + tuple(ends)

        def members_a(group):
            return tuple(d for k in group for d in ((0,) if k == 0 else (-step, step) if k == 1 else (2,)))

        def members_b(group):
            return tuple(d for k in group for d in ((0,) if k == 0 else (-step * k, step * k) if k < 4 else (4,)))

        second_a = ring(
            (label, "a", "z"), "z", tuple(members_a(g) for g in groups_a),
            lambda i, d, s=span_a: slab.at[i, lax.rem(x + d + NX, NX), s, :], bytes_a, p, size_a)
        second_b = ring(
            (label, "b", "x"), "x", tuple(members_b(g) for g in groups_b),
            lambda i, d, s=span_b: slab.at[lax.rem(z + d + NZ, NZ), i, s, :], bytes_b, p, size_b)
        done_a = first_ring(
            "a", "x", lambda i, _, s=span_a: slab.at[z, i, s, :], size_a, bytes_a, second_a, groups_a)
        done_b = first_ring(
            "b", "z", lambda i, _, s=span_b: slab.at[i, x, s, :], size_b,
            lambda ways, width, s=span_b: slab.at[pl.ds(0, ways), pl.ds(0, width), s, :], second_b, groups_b)
        piece_done[label] = done_a + done_b
        if p:
            for task in tasks:
                if task.name in ((label, "a", "x", "start"), (label, "b", "z", "start")):
                    task.after = task.after + ((PIECES[p - 1][0],) + task.name[1:],)

    held = {1: x1, 2: h1, 3: x2, 4: mixed, 5: x3, 6: h2}
    share_sems = {stage: take() for stage in held}
    for stage, ref in held.items():
        drains.append((ref.at[pl.ds(0, 7)], share_sems[stage]))
    up, down, partner = toward("y", NY, y, step), toward("y", NY, y, -step), {"c": 1 - c}

    def slot_at(distance):
        return lax.rem(y + distance + NY, NY) * 2 + c

    def part_of(stage, unit, slots):
        row, rows, first, lanes = UNITS[stage][unit]
        return held[stage].at[slots, row : row + rows, first : first + lanes]

    def share(stage, unit, slot, hops):
        for tag, device in hops:
            send((stage, unit, tag), share_sems[stage], part_of(stage, unit, slot), device)

    def share_own(stage, unit):
        share(stage, unit, me, (("near", up), ("near", down), ("d", partner)))

    def unit_size(stage, unit):
        return UNITS[stage][unit][1] * UNITS[stage][unit][3] * 2

    def own_sends(stage, unit):
        size = unit_size(stage, unit)
        return [((stage, unit, "f1"), "yf", size), ((stage, unit, "b1"), "yb", size), ((stage, unit, "d0"), "d", size)]

    def share_tasks(stage, unit):
        size = unit_size(stage, unit)

        def first():
            await_bytes(part_of(stage, unit, pl.ds(0, 2)), recv_of[(stage, unit, "near")])
            share(stage, unit, slot_at(-step), (("far", up), ("d", partner)))
            share(stage, unit, slot_at(step), (("d", partner),))

        def second():
            await_bytes(part_of(stage, unit, 0), recv_of[(stage, unit, "far")])
            share(stage, unit, slot_at(2), (("d", partner),))

        add((stage, unit, "first"), first, needs=((stage, unit, "f1"), (stage, unit, "b1")), rank=-2, cost=0.1,
            sends=[((stage, unit, "f2"), "yf", size), ((stage, unit, "d1"), "d", size), ((stage, unit, "d2"), "d", size)])
        add((stage, unit, "second"), second, after=((stage, unit, "first"),), needs=((stage, unit, "f2"),), rank=-2,
            sends=[((stage, unit, "d3"), "d", size)])

    def rows_of(chunk):
        return slice(chunk * SEQ_LEN, (chunk + 1) * SEQ_LEN)

    def weight(name, first, count):
        unit = UNIT[name]
        parts = []
        for tile in range(first, first + count):
            start = OFFSET[name] + unit * tile
            parts.append(slab[:, :, start : start + unit, :].reshape(NZ * NX * unit, LANES))
        return jnp.concatenate(parts, axis=1)

    def normalized(ref, chunk, gain, width):
        squares = jnp.zeros((SEQ_LEN, LANES), F32)
        for slot in range(TP):
            value = ref[slot, rows_of(chunk), :].astype(F32)
            wide[rows_of(chunk), slot * width : (slot + 1) * width] = (
                value * gain[:, slot * width : (slot + 1) * width]
            ).astype(BF16)
            square = value * value
            for lane_tile in range(width // LANES):
                squares = squares + square[:, lane_tile * LANES : (lane_tile + 1) * LANES]
        mean = jnp.sum(squares, axis=1, keepdims=True) * (1.0 / (TP * width))
        factor = jnp.broadcast_to(lax.rsqrt(mean + EPSILON), (SEQ_LEN, LANES))
        factors[rows_of(chunk), :] = factor
        return factor

    def product(lhs, name, first, count):
        return jnp.dot(lhs, weight(name, first, count), preferred_element_type=F32)

    def up_unit(name, target, unit):
        row, rows, first, lanes = unit
        span = slice(row, row + rows)
        factor = factors[span, :]
        for tile in range(first // LANES, (first + lanes) // LANES):
            both = product(wide[span, :], name, 2 * tile, 2)
            target[me, span, tile * LANES : (tile + 1) * LANES] = (
                silu(both[:, :LANES] * factor) * (both[:, LANES:] * factor)
            ).astype(BF16)

    def down_stage(source, name, residual, finish):
        def run(chunk):
            lhs = jnp.concatenate([source[slot, rows_of(chunk), :] for slot in range(TP)], axis=1)
            total = product(lhs, name, 0, 2)
            finish(chunk, (residual[me, rows_of(chunk), :].astype(F32) + 0.5 * total).astype(BF16))
        return run

    def finish_into(target):
        def finish(chunk, value):
            target[me, rows_of(chunk), :] = value
        return finish

    def finish_out(chunk, value):
        out[rows_of(chunk), :] = value

    def mix_stage(chunk):
        factor = normalized(x2, chunk, mix_gain, 256)
        both = product(wide[rows_of(chunk), :], W3, 0, 2)
        branch, gate_act = both[:, :LANES] * factor, both[:, LANES:] * factor
        time = lax.broadcasted_iota(jnp.int32, (SEQ_LEN, LANES), 0)

        def earlier(value, k, fill):
            return jnp.where(time >= k, pltpu.roll(value, k, 0), fill)

        convolved = jnp.zeros((SEQ_LEN, LANES), F32)
        for k in range(4):
            lag = 3 - k
            shifted = branch if lag == 0 else earlier(branch, lag, 0.0)
            convolved = convolved + shifted * taps[k : k + 1, :]
        convolved = convolved.astype(BF16)
        retained = sigmoid(jnp.dot(convolved, blocks[0], preferred_element_type=F32))
        admitted = sigmoid(jnp.dot(convolved, blocks[1], preferred_element_type=F32))
        rate = DECAY_SCALE * softplus(-decay[...]) * retained
        add_now = jnp.sqrt(stable_one_minus_exp(2.0 * rate)) * admitted * convolved.astype(F32)
        keep = jnp.exp(-rate)
        k = 1
        while k < SEQ_LEN:
            add_now = keep * earlier(add_now, k, 0.0) + add_now
            if 2 * k < SEQ_LEN:
                keep = keep * earlier(keep, k, 1.0)
            k *= 2
        mixed[me, rows_of(chunk), :] = (add_now * gelu(gate_act)).astype(BF16)

    def out_stage(chunk):
        factor = normalized(mixed, chunk, channel_gain, 128)
        total = product(wide[rows_of(chunk), : TP * LANES], W4, 0, 2) * jnp.concatenate((factor, factor), axis=1)
        x3[me, rows_of(chunk), :] = (x2[me, rows_of(chunk), :].astype(F32) + total).astype(BF16)

    def enter():
        token_load.wait()
        pl.semaphore_wait(barrier, len(neighbours))

    add(("enter",), enter, after=(("build", W1),), rank=-5)
    add(("build", "blocks"), build_blocks, cost=0.3, rank=3, after=(("enter",),))
    first_sends = ((PIECES[0][0], "a", "x", "start"), (PIECES[0][0], "b", "z", "start"))
    for task in tasks:
        if task.name[0] == "build" and task.name[1] != W1:
            task.after = task.after + first_sends
    for unit in range(len(UNITS[1])):
        add(("share", 1, unit), functools.partial(share_own, 1, unit), after=first_sends, sends=own_sends(1, unit), rank=1)
    for stage in held:
        for unit in range(len(UNITS[stage])):
            share_tasks(stage, unit)

    def inputs(stage, chunk):
        row = chunk * SEQ_LEN
        units = [u for u, (r, n, _, _) in enumerate(UNITS[stage]) if r <= row < r + n]
        return units, [(stage, u, "d%d" % n) for u in units for n in range(4)], [(stage, u, "second") for u in units]

    received = set()

    def receive(stage, chunk):
        for unit in inputs(stage, chunk)[0]:
            if (stage, unit) not in received:
                received.add((stage, unit))
                await_bytes(part_of(stage, unit, pl.ds(0, 4)), recv_of[(stage, unit, "d")])

    def add_up(stage, source, gain, name, target, labels):
        for chunk in range(CHUNKS):
            def norm(chunk=chunk):
                receive(stage, chunk)
                normalized(source, chunk, gain, 256)
            _, needs, after = inputs(stage, chunk)
            if stage == 5:
                after = after + [("compute", 4, n) for n in range(CHUNKS)]
            add(("norm", stage, chunk), norm, after=after, needs=needs, cost=COST["norm"], rank=2)
        for u, unit in enumerate(UNITS[stage + 1]):
            row, rows, first, lanes = unit
            def run(u=u, unit=unit):
                up_unit(name, target, unit)
                share_own(stage + 1, u)
            pieces = labels[first // LANES : (first + lanes) // LANES]
            after = [t for piece in pieces for t in piece_done[piece]]
            after += [("norm", stage, n) for n in range(row // SEQ_LEN, (row + rows) // SEQ_LEN)]
            add(("tile", stage, u), run, after=after, sends=own_sends(stage + 1, u), rank=-1,
                cost=COST["tile"] * rows * lanes / (SEQ_LEN * LANES))

    def add_rows(stage, run, piece, before=()):
        for chunk in range(CHUNKS):
            def compute(chunk=chunk):
                receive(stage, chunk)
                run(chunk)
                if stage < 6:
                    share_own(stage + 1, chunk)
            _, needs, after = inputs(stage, chunk)
            after = after + list(piece_done[piece]) + list(before(chunk) if before else ())
            add(("compute", stage, chunk), compute, after=after, needs=needs, rank=-1, cost=COST[stage],
                sends=own_sends(stage + 1, chunk) if stage < 6 else ())

    add_up(1, x1, pre_gain, W1, h1, ("1a", "1b", "1c"))
    add_rows(2, down_stage(h1, W2, x1, finish_into(x2)), "2")
    add_rows(3, mix_stage, "34", lambda chunk: [("build", "blocks")] + [("tile", 1, u) for u in range(len(UNITS[2]))])
    add_rows(4, out_stage, "34")
    add_up(5, x3, post_gain, W5, h2, ("5", "5", "5"))
    add_rows(6, down_stage(h2, W6, x3, finish_out), "6")

    for task in ordered(tasks):
        task.fn()
    for ref, sem in drains:
        await_bytes(ref, sem)
    assert used["recv"] <= SEMS, used["recv"]


def layer(
    tokens, pre_gain, pre_gate, pre_up, pre_down, mix_gain, branch_proj, gate_proj, conv_taps,
    retain_blocks, admit_blocks, decay_param, channel_gain, out_proj, post_gain, post_gate,
    post_up, post_down,
):
    large = (tokens, pre_gate, pre_up, pre_down, branch_proj, gate_proj, out_proj, post_gate, post_up, post_down)
    small = (
        pre_gain.reshape(1, -1), mix_gain.reshape(1, -1), channel_gain.reshape(1, -1),
        post_gain.reshape(1, -1), conv_taps, retain_blocks, admit_blocks, decay_param.reshape(1, -1),
    )
    return pl.pallas_call(
        kernel,
        out_shape=jax.ShapeDtypeStruct(tokens.shape, tokens.dtype),
        in_specs=[pl.BlockSpec(memory_space=pl.ANY)] * len(large)
        + [pl.BlockSpec(memory_space=pltpu.VMEM)] * len(small),
        out_specs=pl.BlockSpec(memory_space=pltpu.VMEM),
        scratch_shapes=[pltpu.VMEM(a.shape, F32) for a in large[1:]]
        + [
            pltpu.VMEM((NZ, NX, SLAB, LANES), BF16),
            pltpu.VMEM((TP, ROWS, 256), BF16),
            pltpu.VMEM((TP, ROWS, 256), BF16),
            pltpu.VMEM((TP, ROWS, 256), BF16),
            pltpu.VMEM((TP, ROWS, 384), BF16),
            pltpu.VMEM((TP, ROWS, 384), BF16),
            pltpu.VMEM((TP, ROWS, 128), BF16),
            pltpu.VMEM((ROWS, 2048), BF16),
            pltpu.VMEM((ROWS, LANES), F32),
            pltpu.VMEM((352, 384), BF16),
            pltpu.VMEM((2, LANES, LANES), BF16),
            pltpu.SemaphoreType.DMA((len(large),)),
            pltpu.SemaphoreType.DMA((SEMS,)),
        ],
        compiler_params=pltpu.CompilerParams(
            collective_id=0, has_side_effects=True, vmem_limit_bytes=56 * 1024 * 1024
        ),
        name="layer",
    )(*large, *small)


def solution(mesh):
    torus = Mesh(mesh.devices.reshape(NZ, NX, NY, 2), ("z", "x", "y", "c"))
    fs, tp = ("z", "x"), ("y", "c")
    split = P(fs, tp)
    placed = (
        split, P(), split, split, split, P(), split, split, P(None, tp), P(tp, None, None),
        P(tp, None, None), P(tp), P(), split, P(), split, split, split,
    )
    return jax.shard_map(layer, mesh=torus, in_specs=placed, out_specs=split, check_vma=False)
```

time: 138 us -> 119 us (0.86)
  Pallas kernels: 136 us -> 117 us
    pallas_call x1, Pallas kernels: 136 us -> 117 us  [layer(): pl.pallas_call(kernel, out_shape=jax.ShapeDtypeStruct(tokens.shape, token...]
where the time goes in v2:
time: 119 us
  Pallas kernels  117 us (98%)
  local copies, waits for them, and re-layouts  1.67 us (1%)
    pallas_call x1, Pallas kernels, layer(): pl.pallas_call(kernel, out_shape=jax.ShapeDtypeStruct(tokens.shape, token...  117 us

profile of v2, /device:TPU:1, one launch (start us, length us, event | category | flops | bytes accessed | tf_op | source)
XLA Modules:
  0.0 119.0 jit_solution(10524703927712083944)
XLA Ops:
  0.0 117.3 %layer.1 = bf16[512,256]{1,0:T(8,128)(2,1)} custom-call(bf16[512,256]{1,0:T(8,128)(2,1)} %tokens.1, f32[64,352]{1,0:T(8,128)} %pre_gate.1, f32[64,352]{1,0:T(8,128)} %pre_up.1, f32[88,256]{1,0:T(8,128)} %pre_down.1, f32[64,128]{1,0:T(8,128)} %branch_proj.1, f32[64,128]{1,0:T(8,128)} %gate_proj.1, f32[32,256]{1,0:T(8,128)} %out_proj.1, f32[64,352]{1,0:T(8,128)} %post_gate.1, ...), custom_call_target="tpu_custom_call" | custom-call | tf_op jit(solution)/shard_map/layer/pallas_call | solution.py:623
  117.3 1.7 %copy.20 = bf16[512,256]{1,0:T(8,128)(2,1)} copy(bf16[512,256]{1,0:T(8,128)(2,1)} %layer.1) | data formatting | bytes 524288

commit v3 on v2

--- a/solution.py
+++ b/solution.py
@@ -51,17 +51,33 @@
     6: tuple((r, n, 0, 384) for r, n in QUARTERS),
 }
 
-SEMS = 320
+SEMS = 258
 LINK_RATE, CHIP_RATE = 91e3, 500e3
-LINK_LATENCY, CHIP_LATENCY = 1.8, 1.0
-BACKLOG = 60e3
-COST = {"norm": 0.25, "tile": 0.2, 2: 0.55, 3: 0.8, 4: 0.3, 6: 0.55}
+LINK_LATENCY, CHIP_LATENCY = 3.00, 1.0
+HOLD, MARGIN = 100000, 0
+GATES = {
+    "a1a": ("z", 1000000),
+    "a1b": ("z", 1000000),
+    "a1c": ("z", 4000000),
+    "a2": ("z", 1000000),
+    "a34": ("z", 500000),
+    "a5": ("z", 1000000),
+    "a6": ("x", 356000),
+    "b1a": ("z", 500000),
+    "b1b": ("z", 700000),
+    "b1c": ("z", 3400000),
+    "b2": ("x", 1200000),
+    "b34": ("z", 866000),
+    "b5": ("x", 1000000),
+    "b6": ("z", 364000),
+}
+COST = {"norm": 0.23, "tile": 0.2, 2: 0.57, 3: 0.8, 4: 0.3, 6: 0.55}
 
 
 class Task:
-    def __init__(self, name, fn, after=(), needs=(), sends=(), cost=0.05, rank=0, gate=None):
+    def __init__(self, name, fn, after=(), needs=(), sends=(), cost=0.05, rank=0, gate=None, held=False):
         self.name, self.fn, self.after, self.needs = name, fn, tuple(after), tuple(needs)
-        self.sends, self.cost, self.rank, self.gate = tuple(sends), cost, rank, gate
+        self.sends, self.cost, self.rank, self.gate, self.held = tuple(sends), cost, rank, gate, held
 
 
 class Links:
@@ -94,28 +110,45 @@
                     self.queues[q].pop(0)
                     self.arrival[head[0]] = self.now + latency
 
+    def backlog(self, axis):
+        return sum(size for q in (axis + "f", axis + "b") for _, size in self.queues.get(q, ()))
+
     def next_event(self):
-        times = [t for t in self.arrival.values() if t > self.now + 1e-9]
+        times = [t + m for t in self.arrival.values() for m in (0.0, MARGIN) if t + m > self.now + 1e-9]
         times += [self.now + self.queues[q][0][1] / rate + 1e-6 for q, rate, _ in self.flows()]
         return min(times)
 
-    def backlog(self, axis):
-        return sum(size for q in (axis + "f", axis + "b") for _, size in self.queues.get(q, ()))
-
 
 def ordered(tasks):
     links, done, order, left = Links(), set(), [], list(tasks)
-    waiting = {}
     trace = []
+    pieces = [piece[0] for piece in PIECES]
+    work = {}
+    for task in tasks:
+        for message, queue, size in task.sends:
+            work[message] = (message[0][0] if isinstance(message[0], tuple) else None, queue[0], size)
+
+    def shut(gate):
+        axis, label, limit = gate
+        earlier = pieces[: pieces.index(label)]
+        rest = sum(
+            size for m, (piece, a, size) in work.items() if a == axis and piece in earlier and m not in links.arrival)
+        return rest > limit
+
     while left:
         best = None
+        lead = min((task.rank for task in left if task.held), default=0)
         for task in left:
             if not all(a in done for a in task.after):
+                continue
+            if task.held and task.rank > lead and any(links.backlog(q[0]) > HOLD for _, q, _ in task.sends):
                 continue
             ready = 0.0
             for m in task.needs:
                 ready = max(ready, links.arrival.get(m, 1e9))
-            if ready > links.now or (task.gate and links.backlog(task.gate) > BACKLOG):
+            if task.held and task.needs and task.rank > 2:
+                ready += MARGIN
+            if ready > links.now or (task.gate and shut(task.gate)):
                 continue
             if best is None or (task.rank, ready) < best[0]:
                 best = ((task.rank, ready), task)
@@ -165,9 +198,10 @@
 
 def kernel(
     tokens, pre_gate, pre_up, pre_down, branch_proj, gate_proj, out_proj, post_gate, post_up,
-    post_down, pre_gain, mix_gain, channel_gain, post_gain, taps, retain, admit, decay,
+    post_down, h_pre_gain, h_mix_gain, h_channel_gain, h_post_gain, h_taps, h_retain, h_admit, h_decay,
     out,
     s_pre_gate, s_pre_up, s_pre_down, s_branch, s_gate, s_out, s_post_gate, s_post_up, s_post_down,
+    pre_gain, mix_gain, channel_gain, post_gain, taps, retain, admit, decay, result,
     slab, x1, x2, x3, h1, h2, mixed, wide, factors, spread, blocks, local_sem, sems,
 ):
     z, x, y, c = (lax.axis_index(a) for a in ("z", "x", "y", "c"))
@@ -180,13 +214,21 @@
         "gate": (gate_proj, s_gate), "out": (out_proj, s_out),
         "post_gate": (post_gate, s_post_gate), "post_up": (post_up, s_post_up),
         "post_down": (post_down, s_post_down),
+        "pre_gain": (h_pre_gain, pre_gain), "mix_gain": (h_mix_gain, mix_gain),
+        "channel_gain": (h_channel_gain, channel_gain), "post_gain": (h_post_gain, post_gain),
+        "taps": (h_taps, taps), "retain": (h_retain, retain), "admit": (h_admit, admit), "decay": (h_decay, decay),
     }
     loads = {}
     for n, (key, (src, dst)) in enumerate(shards.items()):
         loads[key] = pltpu.make_async_copy(src, dst, local_sem.at[n])
         loads[key].start()
-    token_load = pltpu.make_async_copy(tokens, x1.at[me], local_sem.at[len(shards)])
-    token_load.start()
+    loads["tokens"] = pltpu.make_async_copy(tokens, x1.at[me], local_sem.at[len(shards)])
+    loads["tokens"].start()
+
+    def loaded(*keys):
+        for key in keys:
+            if key in loads:
+                loads.pop(key).wait()
 
     def toward(axis, n, index, distance):
         return {axis: lax.rem(index + distance + n, n)}
@@ -229,29 +271,30 @@
 
     def build_wide(name, gate_key, up_key):
         for half, key in enumerate((gate_key, up_key)):
-            loads[key].wait()
+            loaded(key)
             placed = jnp.dot(shards[key][1][...].astype(BF16), spread[...], preferred_element_type=F32)
             for tile in range(3):
                 put(name, half + 2 * tile, placed[:, tile * LANES : (tile + 1) * LANES])
 
     def build_down(name, key):
-        loads[key].wait()
+        loaded(key)
         for tile in range(2):
             value = shards[key][1][:, tile * LANES : (tile + 1) * LANES]
             put(name, tile, jnp.concatenate((value, jnp.zeros((8, LANES), F32)), axis=0))
 
     def build_mixer():
-        loads["branch"].wait()
+        loaded("branch")
         put(W3, 0, s_branch[...])
-        loads["gate"].wait()
+        loaded("gate")
         put(W3, 1, s_gate[...])
 
     def build_out():
-        loads["out"].wait()
+        loaded("out")
         for tile in range(2):
             put(W4, tile, s_out[:, tile * LANES : (tile + 1) * LANES])
 
     def build_blocks():
+        loaded("retain", "admit")
         tall = lax.broadcasted_iota(jnp.int32, (LANES, 64), 0)
         flat = lax.broadcasted_iota(jnp.int32, (LANES, 64), 1)
         wide_r = lax.broadcasted_iota(jnp.int32, (64, LANES), 0)
@@ -314,7 +357,7 @@
                 starts_k = relay
                 ring_tasks[(label, g, k)] = Task(
                     (label, g, k), relay, after=((label, g, k - 1),), needs=needs, rank=rank,
-                    sends=queued(k + 1) if k < far else (), cost=0.07)
+                    sends=queued(k + 1) if k < far else (), cost=0.03, held=True)
 
             def begin(hop=hop):
                 hop("f", 1)
@@ -359,7 +402,7 @@
                 begin()
                 launch(0)
 
-            add(key, starting, after=ready, rank=p, sends=list(queued) + launch_sends(0), cost=0.1, gate=axis)
+            add(key, starting, after=ready, rank=p, sends=list(queued) + launch_sends(0), cost=0.04, gate=(GATES[part + label][0], label, GATES[part + label][1]), held=True)
             previous, last = key, None
             for k, name in enumerate(names, 1):
                 task = ring_tasks[name]
@@ -368,7 +411,7 @@
                     inner()
                     launch(k)
 
-                add(name, run, after=(previous,), needs=task.needs, rank=p, cost=0.1,
+                add(name, run, after=(previous,), needs=task.needs, rank=p, cost=0.04, held=True,
                     sends=task.sends + tuple(launch_sends(k)))
                 previous = name
             ends = []
@@ -377,7 +420,7 @@
                 for k, name in enumerate(second[g][2], 1):
                     task = ring_tasks[name]
                     add(name, task.fn, after=(begun if k == 1 else second[g][2][k - 2],), needs=task.needs,
-                        rank=p, sends=task.sends, cost=0.07)
+                        rank=p, sends=task.sends, cost=0.03, held=True)
                 ends.append(second[g][2][-1])
             return (previous,) + tuple(ends)
 
@@ -459,7 +502,8 @@
             parts.append(slab[:, :, start : start + unit, :].reshape(NZ * NX * unit, LANES))
         return jnp.concatenate(parts, axis=1)
 
-    def normalized(ref, chunk, gain, width):
+    def normalized(ref, chunk, gain, width, key):
+        loaded(key)
         squares = jnp.zeros((SEQ_LEN, LANES), F32)
         for slot in range(TP):
             value = ref[slot, rows_of(chunk), :].astype(F32)
@@ -499,12 +543,18 @@
             target[me, rows_of(chunk), :] = value
         return finish
 
+    stores = []
+
     def finish_out(chunk, value):
-        out[rows_of(chunk), :] = value
+        result[rows_of(chunk), :] = value
+        stores.append(pltpu.make_async_copy(
+            result.at[rows_of(chunk), :], out.at[rows_of(chunk), :], local_sem.at[len(shards) + 1 + chunk]))
+        stores[-1].start()
 
     def mix_stage(chunk):
-        factor = normalized(x2, chunk, mix_gain, 256)
+        factor = normalized(x2, chunk, mix_gain, 256, "mix_gain")
         both = product(wide[rows_of(chunk), :], W3, 0, 2)
+        loaded("taps", "decay")
         branch, gate_act = both[:, :LANES] * factor, both[:, LANES:] * factor
         time = lax.broadcasted_iota(jnp.int32, (SEQ_LEN, LANES), 0)
 
@@ -531,12 +581,12 @@
         mixed[me, rows_of(chunk), :] = (add_now * gelu(gate_act)).astype(BF16)
 
     def out_stage(chunk):
-        factor = normalized(mixed, chunk, channel_gain, 128)
+        factor = normalized(mixed, chunk, channel_gain, 128, "channel_gain")
         total = product(wide[rows_of(chunk), : TP * LANES], W4, 0, 2) * jnp.concatenate((factor, factor), axis=1)
         x3[me, rows_of(chunk), :] = (x2[me, rows_of(chunk), :].astype(F32) + total).astype(BF16)
 
     def enter():
-        token_load.wait()
+        loaded("tokens")
         pl.semaphore_wait(barrier, len(neighbours))
 
     add(("enter",), enter, after=(("build", W1),), rank=-5)
@@ -568,7 +618,7 @@
         for chunk in range(CHUNKS):
             def norm(chunk=chunk):
                 receive(stage, chunk)
-                normalized(source, chunk, gain, 256)
+                normalized(source, chunk, gain, 256, "pre_gain" if stage == 1 else "post_gain")
             _, needs, after = inputs(stage, chunk)
             if stage == 5:
                 after = after + [("compute", 4, n) for n in range(CHUNKS)]
@@ -582,7 +632,7 @@
             after = [t for piece in pieces for t in piece_done[piece]]
             after += [("norm", stage, n) for n in range(row // SEQ_LEN, (row + rows) // SEQ_LEN)]
             add(("tile", stage, u), run, after=after, sends=own_sends(stage + 1, u), rank=-1,
-                cost=COST["tile"] * rows * lanes / (SEQ_LEN * LANES))
+                cost=COST["tile"] * (1.0 + rows * lanes / (SEQ_LEN * LANES)))
 
     def add_rows(stage, run, piece, before=()):
         for chunk in range(CHUNKS):
@@ -607,6 +657,8 @@
         task.fn()
     for ref, sem in drains:
         await_bytes(ref, sem)
+    for store in stores:
+        store.wait()
     assert used["recv"] <= SEMS, used["recv"]
 
 
@@ -623,11 +675,11 @@
     return pl.pallas_call(
         kernel,
         out_shape=jax.ShapeDtypeStruct(tokens.shape, tokens.dtype),
-        in_specs=[pl.BlockSpec(memory_space=pl.ANY)] * len(large)
-        + [pl.BlockSpec(memory_space=pltpu.VMEM)] * len(small),
-        out_specs=pl.BlockSpec(memory_space=pltpu.VMEM),
-        scratch_shapes=[pltpu.VMEM(a.shape, F32) for a in large[1:]]
+        in_specs=[pl.BlockSpec(memory_space=pl.ANY)] * (len(large) + len(small)),
+        out_specs=pl.BlockSpec(memory_space=pl.ANY),
+        scratch_shapes=[pltpu.VMEM(a.shape, F32) for a in large[1:] + small]
         + [
+            pltpu.VMEM(tokens.shape, BF16),
             pltpu.VMEM((NZ, NX, SLAB, LANES), BF16),
             pltpu.VMEM((TP, ROWS, 256), BF16),
             pltpu.VMEM((TP, ROWS, 256), BF16),
@@ -639,7 +691,7 @@
             pltpu.VMEM((ROWS, LANES), F32),
             pltpu.VMEM((352, 384), BF16),
             pltpu.VMEM((2, LANES, LANES), BF16),
-            pltpu.SemaphoreType.DMA((len(large),)),
+            pltpu.SemaphoreType.DMA((len(large) + len(small) + CHUNKS,)),
             pltpu.SemaphoreType.DMA((SEMS,)),
         ],
         compiler_params=pltpu.CompilerParams(

time: 119 us -> 102 us (0.86)
  Pallas kernels: 117 us -> 100 us
    pallas_call x1, Pallas kernels: 117 us -> 100 us  [layer(): pl.pallas_call(kernel, out_shape=jax.ShapeDtypeStruct(tokens.shape, token...]
where the time goes in v3:
time: 102 us
  Pallas kernels  100 us (98%)
  local copies, waits for them, and re-layouts  1.67 us (2%)
    pallas_call x1, Pallas kernels, layer(): pl.pallas_call(kernel, out_shape=jax.ShapeDtypeStruct(tokens.shape, token...  100 us

profile of v3, /device:TPU:1, one launch (start us, length us, event | category | flops | bytes accessed | tf_op | source)
XLA Modules:
  0.0 102.2 jit_solution(8621579532686128189)
XLA Ops:
  0.0 100.5 %layer.1 = bf16[512,256]{1,0:T(8,128)(2,1)} custom-call(bf16[512,256]{1,0:T(8,128)(2,1)} %tokens.1, f32[64,352]{1,0:T(8,128)} %pre_gate.1, f32[64,352]{1,0:T(8,128)} %pre_up.1, f32[88,256]{1,0:T(8,128)} %pre_down.1, f32[64,128]{1,0:T(8,128)} %branch_proj.1, f32[64,128]{1,0:T(8,128)} %gate_proj.1, f32[32,256]{1,0:T(8,128)} %out_proj.1, f32[64,352]{1,0:T(8,128)} %post_gate.1, ...), custom_call_target="tpu_custom_call" | custom-call | tf_op jit(solution)/shard_map/layer/pallas_call | solution.py:675
  100.5 1.7 %copy.20 = bf16[512,256]{1,0:T(8,128)(2,1)} copy(bf16[512,256]{1,0:T(8,128)(2,1)} %layer.1) | data formatting | bytes 524288
